TPU v7x, 32 devices: a whole 2x2x4 slice. The times are simulated.
32 devices in a mesh: sp: 16 (over z, y, x), tp: 2 (over core).
Axes of the slice: x: 2, y: 2, z: 4, core: 2. Of those that a mesh axis runs over, the one named last changes fastest.
Arguments:
- stream: bfloat16 [4096, 2048], P('sp', 'tp'), may hold values from -6 to 6
- out_grad: bfloat16 [4096, 2048], P('sp', 'tp'), may hold values from -6 to 6
- gate_in: bfloat16 [4096, 1024], P('sp', 'tp'), may hold values from -6 to 6
- conv_gate: bfloat16 [4096, 1024], P('sp', 'tp'), may hold values from -6 to 6
- conv_value: bfloat16 [4096, 1024], P('sp', 'tp'), may hold values from -6 to 6
- taps: float32 [3, 1024], P(None, 'tp'), may hold values from -3.5 to 3.5
- w_out: bfloat16 [2048, 1024], P(None, 'tp'), may hold values from -0.1875 to 0.1875
- route_ids: int32 [4096, 2], P('sp'), may hold values from 0 to 15, all different within a row; in each aligned block of 256 rows (0 to 255, 256 to 511, ...) at most 64 rows name the same one
- route_weights: float32 [4096, 2], P('sp'), may hold values from 0.1 to 1
- w_gate: bfloat16 [16, 2048, 1024], P('sp', None, 'tp'), may hold values from -0.125 to 0.125
- w_up: bfloat16 [16, 2048, 1024], P('sp', None, 'tp'), may hold values from -0.125 to 0.125
- w_down: bfloat16 [16, 1024, 2048], P('sp', 'tp'), may hold values from -0.1875 to 0.1875
Outputs:
- stream_grad: bfloat16 [4096, 2048], P('sp', 'tp')
- gate_in_grad: bfloat16 [4096, 1024], P('sp', 'tp')
- conv_gate_grad: bfloat16 [4096, 1024], P('sp', 'tp')
- conv_value_grad: bfloat16 [4096, 1024], P('sp', 'tp')
- w_out_grad: float32 [2048, 1024], P('sp', 'tp')
- w_gate_grad: float32 [16, 2048, 1024], P('sp', None, 'tp')
- w_up_grad: float32 [16, 2048, 1024], P('sp', None, 'tp')
- w_down_grad: float32 [16, 1024, 2048], P('sp', 'tp')
Inputs may be any that keep to these rules, and one draw needn't show every extreme that they name: `route_ids`: the ids of one token differ. Within each aligned block of 256 tokens (the rows of one index of sp), no expert is named by more than 64 routes, and in every draw some expert is named by exactly 64 routes of some block.
All inputs are finite; a program needn't handle non-finite values.
Results may differ from a plain program's by a relative error of at most 0.009.
Values may be sent and summed in bfloat16 or wider, within the bound.
A program may use at most 128 MiB of HBM per device.

v0:
```python
import functools

import jax
import jax.numpy as jnp
from jax import lax
from jax.experimental import pallas as pl
from jax.experimental.pallas import tpu as pltpu
from jax.sharding import PartitionSpec as P

MESH = pl.DeviceIdType.MESH
GROUPS = 4
F32 = jnp.float32
BF16 = jnp.bfloat16


def passed_along(shard, axis, by):
    count = lax.axis_size(axis)
    pairs = [(i, i + by) for i in range(count) if 0 <= i + by < count]
    return lax.ppermute(shard, axis, pairs)


def dot(a, b, ca, cb):
    return lax.dot_general(a, b, (((ca,), (cb,)), ((), ())), preferred_element_type=F32)


def team_size(count):
    size = 1
    while size * size < count:
        size *= 2
    return size


def expert_kernel(
    count,
    cap,
    send_rows,
    send_cot,
    wg_hbm,
    wu_hbm,
    wd_hbm,
    mix_in,
    stream_in,
    grad_in,
    pick,
    scale,
    back_out,
    cross_out,
    mix_out,
    gate_out,
    up_out,
    down_out,
    rows,
    cot,
    wg,
    wu,
    wd,
    pre_g,
    pre_u,
    hidden,
    gg,
    ug,
    part_out,
    part_in,
    ret,
    back,
    gate_f,
    up_f,
    down_f,
    mix,
    toks_in,
    rel_rows,
    rel_cot,
    cross_src,
    cross_dst,
    x_send,
    x_recv,
    w_sem,
    out_sem,
    send_sem,
    recv_sem,
    fsend_sem,
    frecv_sem,
    psend_sem,
    precv_sem,
    rsend_sem,
    rrecv_sem,
    msend_sem,
    mrecv_sem,
):
    me = lax.axis_index("sp")
    half = lax.axis_index("tp")
    other = 1 - half
    per = count // GROUPS
    height = per * cap
    width = rows.shape[2]
    ring = count // 2
    loc = lax.rem(me, ring)
    base = me - loc
    mirror = (lax.rem(me + ring, count), half)

    loads = []
    for n, (a, b) in enumerate(((wg_hbm, wg), (wu_hbm, wu), (wd_hbm, wd))):
        load = pltpu.make_async_copy(a.at[0], b, w_sem.at[n])
        load.start()
        loads.append(load)

    barrier = pltpu.get_barrier_semaphore()

    @pl.loop(1, ring)
    def _(k):
        pl.semaphore_signal(
            barrier, inc=1, device_id=(base + lax.rem(loc + k, ring), half), device_id_type=MESH
        )

    pl.semaphore_signal(barrier, inc=1, device_id=(me, other), device_id_type=MESH)
    pl.semaphore_signal(barrier, inc=1, device_id=mirror, device_id_type=MESH)
    pl.semaphore_wait(barrier, ring + 1)

    def block(k):
        return pl.ds(pl.multiple_of(k * cap, cap), cap)

    def out_copy(which, src, dst, k):
        return pltpu.make_async_remote_copy(
            src_ref=src.at[block(lax.rem(k, ring))],
            dst_ref=dst.at[half, block(k)],
            send_sem=send_sem.at[which, k],
            recv_sem=recv_sem.at[which, k],
            device_id=(base + lax.rem(loc + k, ring), half),
            device_id_type=MESH,
        )

    def pass_copy(which, src, k):
        return pltpu.make_async_remote_copy(
            src_ref=src,
            dst_ref=(rows if which == 0 else cot).at[half, block(k)],
            send_sem=fsend_sem.at[which, k],
            recv_sem=frecv_sem.at[which, k],
            device_id=(me, other),
            device_id_type=MESH,
        )

    def back_copy(k):
        return pltpu.make_async_remote_copy(
            src_ref=ret.at[block(k)],
            dst_ref=back.at[block(k)],
            send_sem=rsend_sem.at[k],
            recv_sem=rrecv_sem.at[k],
            device_id=(base + lax.rem(loc - k + 2 * ring, ring), half),
            device_id_type=MESH,
        )

    team = team_size(count)
    place = lax.rem(me, team)
    toks = mix_in.shape[0]

    def mix_copy(j):
        return pltpu.make_async_remote_copy(
            src_ref=mix_in,
            dst_ref=mix.at[pl.ds(pl.multiple_of(j * toks, toks), toks)],
            send_sem=msend_sem.at[j],
            recv_sem=mrecv_sem.at[j],
            device_id=(me - place + lax.rem(place + j, team), half),
            device_id_type=MESH,
        )

    def part_copy(g):
        at = pl.ds(pl.multiple_of(g * height, height), height)
        return pltpu.make_async_remote_copy(
            src_ref=part_out.at[at],
            dst_ref=part_in.at[at],
            send_sem=psend_sem.at[g],
            recv_sem=precv_sem.at[g],
            device_id=(me, other),
            device_id_type=MESH,
        )

    def cross_copy(n, src, dst):
        return pltpu.make_async_remote_copy(
            src_ref=src,
            dst_ref=dst,
            send_sem=x_send.at[n],
            recv_sem=x_recv.at[n],
            device_id=mirror,
            device_id_type=MESH,
        )

    crossing = (
        cross_copy(0, stream_in, toks_in.at[0]),
        cross_copy(1, grad_in, toks_in.at[1]),
        cross_copy(2, cross_src, cross_dst),
    )
    crossing[0].start()
    crossing[1].start()
    pairs = ((send_rows, rows), (send_cot, cot))
    for which, (src, dst) in enumerate(pairs):
        pass_copy(which, src.at[block(0)], 0).start()

        @pl.loop(1, ring)
        def _(k):
            out_copy(which, src, dst, k).start()

    @pl.loop(1, team)
    def _(j):
        mix_copy(j).start()

    mix[pl.ds(0, toks)] = mix_in[...]
    for which, (src, dst) in enumerate(pairs):
        dst[half, pl.ds(0, cap)] = src[pl.ds(0, cap)]
    for which, (rel, dst) in enumerate(((rel_rows, rows), (rel_cot, cot))):
        crossing[which].wait_recv()
        chosen = dot(pick[...], toks_in[which], 1, 0)
        chosen = (chosen if which == 0 else scale[...] * chosen).astype(BF16)
        rel[...] = chosen
        dst[half, pl.ds(ring * cap, cap)] = chosen[:cap]
        pass_copy(which, rel.at[block(0)], ring).start()

        @pl.loop(ring + 1, count)
        def _(k):
            out_copy(which, rel, dst, k).start()

    for load in loads:
        load.wait()

    def gather_group(which, g):
        src, dst = pairs[which]

        @pl.loop(0, per)
        def _(j):
            k = g * per + j

            @pl.when(lax.rem(k, ring) > 0)
            def _():
                out_copy(which, src, dst, k).wait_recv()
                pass_copy(which, dst.at[half, block(k)], k).start()

        @pl.loop(0, per)
        def _(j):
            k = g * per + j
            pass_copy(which, dst.at[half, block(k)], k).wait_recv()

    @pl.loop(0, GROUPS)
    def _(g):
        gather_group(0, g)
        at = pl.ds(pl.multiple_of(g * height, height), height)
        left, right = rows[0, at], rows[1, at]
        pre_g[at] = dot(left, wg[:width], 1, 0) + dot(right, wg[width:], 1, 0)
        pre_u[at] = dot(left, wu[:width], 1, 0) + dot(right, wu[width:], 1, 0)

    mine_at = pl.ds(pl.multiple_of(half * width, width), width)
    other_at = pl.ds(pl.multiple_of(other * width, width), width)

    @pl.loop(0, GROUPS)
    def _(g):
        gather_group(1, g)
        at = pl.ds(pl.multiple_of(g * height, height), height)
        grad = dot(cot[0, at], wd[:, :width], 1, 1) + dot(cot[1, at], wd[:, width:], 1, 1)
        pg, pu = pre_g[at], pre_u[at]
        sig = jax.nn.sigmoid(pg)
        silu = pg * sig
        hidden[at] = (silu * pu).astype(BF16)
        ug_now = (grad * silu).astype(BF16)
        gg_now = (grad * pu * sig * (1.0 + pg * (1.0 - sig))).astype(BF16)
        ug[at] = ug_now
        gg[at] = gg_now
        far = dot(gg_now, wg[other_at], 1, 1) + dot(ug_now, wu[other_at], 1, 1)
        part_out[at] = far.astype(BF16)
        part_copy(g).start()
        near = dot(gg_now, wg[mine_at], 1, 1) + dot(ug_now, wu[mine_at], 1, 1)
        near = near.astype(BF16).astype(F32)
        part_copy(g).wait_recv()
        ret[at] = (near + part_in[at].astype(F32)).astype(BF16)

        @pl.loop(0, per)
        def _(j):
            k = g * per + j

            @pl.when(lax.rem(k, ring) > 0)
            def _():
                back_copy(k).start()

    back[pl.ds(0, cap)] = ret[pl.ds(0, cap)]
    back[pl.ds(ring * cap, cap)] = ret[pl.ds(ring * cap, cap)]

    tile = 256
    per_half = width // tile

    @pl.loop(0, 2 * per_half)
    def _(t):
        h, c = t // per_half, lax.rem(t, per_half)
        cols = pl.ds(pl.multiple_of(c * tile, tile), tile)
        to = pl.ds(pl.multiple_of(t * tile, tile), tile)
        x = rows[h, :, cols].T
        gate_f[to] = dot(x, gg[...], 1, 0).astype(BF16)
        up_f[to] = dot(x, ug[...], 1, 0).astype(BF16)

    stores = [
        pltpu.make_async_copy(gate_f, gate_out.at[0], out_sem.at[0]),
        pltpu.make_async_copy(up_f, up_out.at[0], out_sem.at[1]),
    ]
    for store in stores:
        store.start()

    hid_tile = min(256, hidden.shape[1])

    @pl.loop(0, hidden.shape[1] // hid_tile)
    def _(t):
        to = pl.ds(pl.multiple_of(t * hid_tile, hid_tile), hid_tile)
        x = hidden[:, to].T
        for h in range(2):
            down_f[to, h * width : (h + 1) * width] = dot(x, cot[h], 1, 0).astype(BF16)

    stores.append(pltpu.make_async_copy(down_f, down_out.at[0], out_sem.at[2]))
    stores[-1].start()

    @pl.loop(ring + 1, count)
    def _(k):
        back_copy(k).wait_recv()

    cross_src[...] = dot(pick[...], back[ring * cap :], 0, 0).astype(BF16)
    crossing[2].start()

    for which, (src, dst) in enumerate(pairs):

        @pl.loop(0, count)
        def _(k):
            @pl.when(lax.rem(k, ring) > 0)
            def _():
                out_copy(which, src, dst, k).wait_send()

            pass_copy(which, dst.at[half, block(k)], k).wait_send()

    @pl.loop(0, GROUPS)
    def _(g):
        part_copy(g).wait_send()

    @pl.loop(1, ring)
    def _(k):
        back_copy(k).wait_send()
        back_copy(k).wait_recv()

    @pl.loop(ring + 1, count)
    def _(k):
        back_copy(k).wait_send()

    @pl.loop(1, team)
    def _(j):
        mix_copy(j).wait_send()
        mix_copy(j).wait_recv()

    mix_out[...] = mix[...]
    back_out[...] = back[: ring * cap]
    for copy in crossing:
        copy.wait_send()
    crossing[2].wait_recv()
    cross_out[...] = cross_dst[...]
    for store in stores:
        store.wait()


def expert_pass(
    send_rows, send_cot, w_gate, w_up, w_down, mixer_out, stream, out_grad, pick, scale, cap
):
    short, width = send_rows.shape
    tall = 2 * short
    toks = stream.shape[0]
    count = lax.axis_size("sp")
    deep, hid = w_gate.shape[1:]
    team = team_size(count)
    vmem = pl.BlockSpec(memory_space=pltpu.VMEM)
    anywhere = pl.BlockSpec(memory_space=pl.ANY)
    dma = pltpu.SemaphoreType.DMA
    return pl.pallas_call(
        functools.partial(expert_kernel, count, cap),
        out_shape=(
            jax.ShapeDtypeStruct((short, width), BF16),
            jax.ShapeDtypeStruct((toks, width), BF16),
            jax.ShapeDtypeStruct((team * mixer_out.shape[0], mixer_out.shape[1]), BF16),
            jax.ShapeDtypeStruct((1, deep, hid), BF16),
            jax.ShapeDtypeStruct((1, deep, hid), BF16),
            jax.ShapeDtypeStruct((1, hid, deep), BF16),
        ),
        in_specs=[vmem, vmem, anywhere, anywhere, anywhere] + [vmem] * 5,
        out_specs=(vmem, vmem, vmem, anywhere, anywhere, anywhere),
        scratch_shapes=[
            pltpu.VMEM((2, tall, width), BF16),
            pltpu.VMEM((2, tall, width), BF16),
            pltpu.VMEM((deep, hid), BF16),
            pltpu.VMEM((deep, hid), BF16),
            pltpu.VMEM((hid, deep), BF16),
            pltpu.VMEM((tall, hid), F32),
            pltpu.VMEM((tall, hid), F32),
            pltpu.VMEM((tall, hid), BF16),
            pltpu.VMEM((tall, hid), BF16),
            pltpu.VMEM((tall, hid), BF16),
            pltpu.VMEM((tall, width), BF16),
            pltpu.VMEM((tall, width), BF16),
            pltpu.VMEM((tall, width), BF16),
            pltpu.VMEM((tall, width), BF16),
            pltpu.VMEM((deep, hid), BF16),
            pltpu.VMEM((deep, hid), BF16),
            pltpu.VMEM((hid, deep), BF16),
            pltpu.VMEM((team * mixer_out.shape[0], mixer_out.shape[1]), BF16),
            pltpu.VMEM((2, toks, width), BF16),
            pltpu.VMEM((short, width), BF16),
            pltpu.VMEM((short, width), BF16),
            pltpu.VMEM((toks, width), BF16),
            pltpu.VMEM((toks, width), BF16),
            dma((3,)),
            dma((3,)),
            dma((3,)),
            dma((3,)),
            dma((2, count)),
            dma((2, count)),
            dma((2, count)),
            dma((2, count)),
            dma((GROUPS,)),
            dma((GROUPS,)),
            dma((count,)),
            dma((count,)),
            dma((team,)),
            dma((team,)),
        ],
        compiler_params=pltpu.CompilerParams(
            collective_id=0, has_side_effects=True, vmem_limit_bytes=60 * 1024 * 1024
        ),
    )(send_rows, send_cot, w_gate, w_up, w_down, mixer_out, stream, out_grad, pick, scale)


def mixer_kernel(
    count,
    sh,
    w_out_hbm,
    mix,
    gate_in,
    wog_out,
    mg_out,
    halo_out,
    far,
    w_out,
    sg,
    p_send,
    p_recv,
    h_send,
    h_recv,
    w_sem,
    whole_sem,
    gsend_sem,
    grecv_sem,
    fsend_sem,
    frecv_sem,
    own_sem,
    psend_sem,
    precv_sem,
    hsem,
):
    me = lax.axis_index("sp")
    half = lax.axis_index("tp")
    other = 1 - half
    team = team_size(count)
    layers = count // team
    place, layer = lax.rem(me, team), me // team
    toks, width = sh.shape
    per = layers // 2
    blk = width // (team * per)
    load = pltpu.make_async_copy(w_out_hbm, w_out, w_sem)
    load.start()

    def member(j):
        return me - place + lax.rem(place + j, team)

    def floor(i):
        return lax.rem(layer + i, layers) * team + place

    after, before = lax.rem(me + 1, count), lax.rem(me + count - 1, count)
    barrier = pltpu.get_barrier_semaphore()

    def greet(device):
        pl.semaphore_signal(barrier, inc=1, device_id=device, device_id_type=MESH)

    for j in range(1, team):
        greet((member(j), half))
    for i in range(1, layers):
        greet((floor(i), half))
    greet((me, other))
    greet((after, half))
    greet((before, half))
    pl.semaphore_wait(barrier, team - 1 + layers - 1 + 3)

    def remote(src, dst, send, recv, device):
        return pltpu.make_async_remote_copy(
            src_ref=src,
            dst_ref=dst,
            send_sem=send,
            recv_sem=recv,
            device_id=device,
            device_id_type=MESH,
        )

    def cols(j, m):
        at = (lax.rem(place + j, team) + team * m) * blk
        return pl.ds(pl.multiple_of(at, blk), blk)

    def spot(h, m, size):
        return pl.ds(pl.multiple_of((h * per + m) * blk, blk), size)

    def stripe(j):
        return pl.ds(j * toks, toks)

    def piece(j, m):
        return remote(
            sh.at[:, cols(j, m)],
            sg.at[stripe(j), spot(half, m, blk)],
            gsend_sem.at[j, m],
            grecv_sem.at[j, m],
            (member(j), half),
        )

    def own_piece(m):
        return remote(
            sh.at[:, cols(0, m)],
            sg.at[stripe(0), spot(half, m, blk)],
            own_sem.at[0, m],
            own_sem.at[1, m],
            (me, other),
        )

    def handed(j):
        ref = sg.at[stripe(j), spot(half, 0, per * blk)]
        return remote(ref, ref, fsend_sem.at[j], frecv_sem.at[j], (me, other))

    whole = remote(sh, far, whole_sem.at[0], whole_sem.at[1], (me, other))
    whole.start()
    for j in range(1, team):
        for m in range(per):
            piece(j, m).start()
    for m in range(per):
        own_piece(m).start()
        sg[stripe(0), spot(half, m, blk)] = sh[:, cols(0, m)]

    load.wait()
    near_at = pl.ds(pl.multiple_of(half * width, width), width)
    far_at = pl.ds(pl.multiple_of(other * width, width), width)
    grad = dot(sh[...], w_out[near_at], 1, 0)
    whole.wait_recv()
    grad = (grad + dot(far[...], w_out[far_at], 1, 0)).astype(BF16)
    mg_out[...] = grad
    h_send[...] = grad[:8].astype(F32) * gate_in[:8].astype(F32)
    halo = remote(h_send, h_recv, hsem.at[0], hsem.at[1], (before, half))
    halo.start()
    for j in range(1, team):
        for m in range(per):
            piece(j, m).wait_recv()
        handed(j).start()
    for m in range(per):
        own_piece(m).wait_recv()
    for j in range(1, team):
        handed(j).wait_recv()

    def share(i):
        at = pl.ds(pl.multiple_of(lax.rem(layer + i, layers) * blk, blk), blk)
        return dot(sg[:, at].T, mix[...], 1, 0)

    def part(i):
        return remote(
            p_send.at[i], p_recv.at[i], psend_sem.at[i], precv_sem.at[i], (floor(i), half)
        )

    @pl.loop(1, layers)
    def _(i):
        p_send[i] = share(i).astype(BF16)
        part(i).start()

    wog_out[...] = share(0)
    for m in range(per):
        own_piece(m).wait_send()
    whole.wait_send()
    for j in range(1, team):
        for m in range(per):
            piece(j, m).wait_send()
        handed(j).wait_send()
    halo.wait_send()
    halo.wait_recv()
    halo_out[...] = h_recv[...]

    @pl.loop(1, layers)
    def _(i):
        part(i).wait_recv()
        wog_out[...] += p_recv[i].astype(F32)

    @pl.loop(1, layers)
    def _(i):
        part(i).wait_send()


def mixer_pass(stream_half, w_out, mix, gate_in):
    count = lax.axis_size("sp")
    team = team_size(count)
    layers = count // team
    per = layers // 2
    toks, width = stream_half.shape
    deep, chans = w_out.shape
    blk = deep // count
    vmem = pl.BlockSpec(memory_space=pltpu.VMEM)
    dma = pltpu.SemaphoreType.DMA
    return pl.pallas_call(
        functools.partial(mixer_kernel, count),
        out_shape=(
            jax.ShapeDtypeStruct((blk, chans), F32),
            jax.ShapeDtypeStruct((toks, chans), BF16),
            jax.ShapeDtypeStruct((8, chans), F32),
        ),
        in_specs=[vmem, pl.BlockSpec(memory_space=pl.ANY), vmem, vmem],
        out_specs=(vmem, vmem, vmem),
        scratch_shapes=[
            pltpu.VMEM((toks, width), BF16),
            pltpu.VMEM((deep, chans), BF16),
            pltpu.VMEM((team * toks, layers * blk), BF16),
            pltpu.VMEM((layers, blk, chans), BF16),
            pltpu.VMEM((layers, blk, chans), BF16),
            pltpu.VMEM((8, chans), F32),
            pltpu.VMEM((8, chans), F32),
            dma,
            dma((2,)),
            dma((team, per)),
            dma((team, per)),
            dma((team,)),
            dma((team,)),
            dma((2, per)),
            dma((layers,)),
            dma((layers,)),
            dma((2,)),
        ],
        compiler_params=pltpu.CompilerParams(
            collective_id=1, has_side_effects=True, vmem_limit_bytes=32 * 1024 * 1024
        ),
    )(stream_half, w_out, mix, gate_in)


def shards(
    stream,
    out_grad,
    gate_in,
    conv_gate,
    conv_value,
    taps,
    w_out,
    route_ids,
    route_weights,
    w_gate,
    w_up,
    w_down,
):
    tok_rows, half_width = stream.shape
    top_count = route_ids.shape[1]
    experts = w_gate.shape[0] * lax.axis_size("sp")
    capacity = 4 * tok_rows // experts
    route_total = tok_rows * top_count
    slots = experts * capacity
    me = lax.axis_index("sp")
    ring = experts // 2
    away = (route_ids // ring != me // ring).astype(jnp.int32)
    flat = (away * ring + lax.rem(route_ids - me + experts, ring)).reshape(route_total)
    one_hot = flat[:, None] == jnp.arange(experts, dtype=jnp.int32)[None, :]
    order = jnp.arange(route_total, dtype=jnp.int32)
    earlier = (order[:, None] > order[None, :]).astype(BF16)
    ranks = dot(earlier, one_hot.astype(BF16), 1, 0)
    slot_pos = jnp.sum(jnp.where(one_hot, ranks, 0.0), axis=1).astype(jnp.int32)
    slot_of = (flat * capacity + slot_pos).reshape(tok_rows, top_count)
    short = slots // 2
    places = jnp.arange(short, dtype=jnp.int32)

    def placed_by(slot_rows, weight_rows):
        hits = [row[None, :] == places[:, None] for row in slot_rows]
        weights = sum(
            jnp.sum(jnp.where(hit, row[None, :], 0.0), axis=1)
            for hit, row in zip(hits, weight_rows)
        )
        return functools.reduce(jnp.logical_or, hits).astype(BF16), weights[:, None]

    table = jnp.concatenate([(slot_of - short).T.astype(F32), route_weights.T], axis=0)
    across = lax.ppermute(table, "sp", [(i, (i + ring) % experts) for i in range(experts)])
    pick_far, scale_far = placed_by(
        across[:top_count].astype(jnp.int32), across[top_count:]
    )
    pick, slot_weight = placed_by(slot_of.T, route_weights.T)
    send_rows = dot(pick, stream, 1, 0).astype(BF16)
    send_cot = (slot_weight * dot(pick, out_grad, 1, 0)).astype(BF16)
    depth = taps.shape[0]
    channels = conv_gate.shape[1]
    prod_rows = conv_gate.astype(jnp.float32) * conv_value.astype(jnp.float32)
    left_rows = passed_along(prod_rows[tok_rows - depth + 1 :], "sp", 1)
    padded = jnp.concatenate([left_rows, prod_rows], axis=0)
    conv_sum = jnp.zeros((tok_rows, channels), jnp.float32)
    for tap_index in range(depth):
        conv_sum = conv_sum + taps[tap_index][None, :] * padded[tap_index : tap_index + tok_rows]
    mixer_out = (gate_in.astype(jnp.float32) * conv_sum).astype(jnp.bfloat16)
    back, crossed, mix, gate_w_grad, up_w_grad, down_w_grad = expert_pass(
        send_rows,
        send_cot,
        w_gate,
        w_up,
        w_down,
        mixer_out,
        stream,
        out_grad,
        pick_far,
        scale_far,
        capacity,
    )
    input_grad = dot(pick, back, 0, 0) + crossed.astype(F32)
    stream_half = (out_grad.astype(jnp.float32) + input_grad).astype(jnp.bfloat16)
    if w_out.shape[0] // lax.axis_size("sp") % 128 == 0:
        out_proj_grad, mixer_grad, halo = mixer_pass(stream_half, w_out, mix, gate_in)
    else:
        stream_whole = lax.all_gather(stream_half, "tp", axis=1, tiled=True)
        mixer_grad = dot(stream_whole, w_out, 1, 0).astype(BF16)
        out_proj_grad = lax.psum_scatter(
            dot(stream_whole, mixer_out, 0, 0).astype(BF16), "sp", scatter_dimension=0, tiled=True
        ).astype(F32)
        first = mixer_grad[: depth - 1].astype(F32) * gate_in[: depth - 1].astype(F32)
        halo = passed_along(first, "sp", -1)
    mixer_wide = mixer_grad.astype(jnp.float32)
    gate_in_grad = (mixer_wide * conv_sum).astype(jnp.bfloat16)
    conv_inner = mixer_wide * gate_in.astype(jnp.float32)
    right_rows = jnp.where(me == lax.axis_size("sp") - 1, 0.0, halo[: depth - 1])
    padded_back = jnp.concatenate([conv_inner, right_rows], axis=0)
    prod_grad = jnp.zeros((tok_rows, channels), jnp.float32)
    for tap_index in range(depth):
        offset = depth - 1 - tap_index
        prod_grad = prod_grad + taps[tap_index][None, :] * padded_back[offset : offset + tok_rows]
    conv_gate_grad = (prod_grad * conv_value.astype(jnp.float32)).astype(jnp.bfloat16)
    conv_value_grad = (prod_grad * conv_gate.astype(jnp.float32)).astype(jnp.bfloat16)
    return (
        stream_half,
        gate_in_grad,
        conv_gate_grad,
        conv_value_grad,
        out_proj_grad,
        gate_w_grad.astype(F32),
        up_w_grad.astype(F32),
        down_w_grad.astype(F32),
    )


def solution(mesh):
    placed = (
        P("sp", "tp"),
        P("sp", "tp"),
        P("sp", "tp"),
        P("sp", "tp"),
        P("sp", "tp"),
        P(None, "tp"),
        P(None, "tp"),
        P("sp", None),
        P("sp", None),
        P("sp", None, "tp"),
        P("sp", None, "tp"),
        P("sp", "tp", None),
    )
    return jax.shard_map(
        shards,
        mesh=mesh,
        in_specs=placed,
        out_specs=(
            P("sp", "tp"),
            P("sp", "tp"),
            P("sp", "tp"),
            P("sp", "tp"),
            P("sp", "tp"),
            P("sp", None, "tp"),
            P("sp", None, "tp"),
            P("sp", "tp", None),
        ),
        check_vma=False,
    )
```

profile of v0, /device:TPU:29, one launch (start us, length us, event | category | flops | bytes accessed | tf_op | source)
XLA Modules:
  0.0 185.0 jit_solution(8953270812452747253)
XLA Ops:
  0.7 0.8 fusion.30
  1.7 0.3 fusion.2
  2.2 0.7 convert_bitcast_fusion
  3.0 0.7 pad_maximum_fusion.2
  3.7 1.1 convert_multiply_fusion.3
  4.8 3.3 %collective-permute-start = (f32[2,512]{1,0:T(2,128)S(1)}, f32[2,512]{1,0:T(2,128)S(1)}, u32[]{:S(2)}, u32[]{:S(2)}) collective-permute-start(f32[2,512]{1,0:T(2,128)S(1)} %slice.46), channel_id=1, source_target_pairs={{0,2},{2,4},{4,6},{6,8},{8,10},{10,12},{12,14},{14,16},{16,18},{18... | collective-permute-start | bytes 12296 | tf_op jit(solution)/shard_map/ppermute | solution.py:19
  8.1 0.8 fusion.38
  8.9 1.4 convolution_convert_fusion.send_rows
  10.5 1.4 multiply_convert_fusion.send_cot
  12.0 0.8 fusion.19.pick
  12.8 0.2 select_reduce_fusion
  13.1 0.9 copy.70.scale
  13.9 0.9 fusion.11
  14.8 126.5 %shard_map.179 = (bf16[512,1024]{1,0:T(8,128)(2,1)}, bf16[256,1024]{1,0:T(8,128)(2,1)}, bf16[1024,512]{1,0:T(8,128)(2,1)}, bf16[1,2048,512]{2,1,0:T(8,128)(2,1)}...) custom-call(bf16[512,1024]{1,0:T(8,128)(2,1)} %convolution_convert_fusion.send_rows, ...), custom_call_target="tpu_custom_call" | custom-call | tf_op jit(solution)/shard_map/pallas_call | solution.py:372
  141.4 2.0 %fusion.1.sh = bf16[256,1024]{1,0:T(8,128)(2,1)S(1)} fusion(bf16[512,1024]{1,0:T(8,128)(2,1)} %get-tuple-element.17, bf16[256,1024]{1,0:T(8,128)(2,1)} %get-tuple-element.18, bf16[256,1024]{1,0:T(8,128)(2,1)S(1)} %copy-done.11, s32[256]{0:T(256)S(1)} %bitcast.33, s32[256]{0:T(256)S(1)} %bitcast.29), kind=kOutput, calls=%fused_computation.4 | convolution fusion | flops 270139392 | bytes 2623488 | tf_op jit(solution)/shard_map/dot_general | solution.py:23
  143.4 1.4 copy-done.2
  144.8 29.2 %shard_map.180 = (f32[128,512]{1,0:T(8,128)S(1)}, bf16[256,512]{1,0:T(8,128)(2,1)S(1)}, f32[8,512]{1,0:T(8,128)S(1)}) custom-call(bf16[256,1024]{1,0:T(8,128)(2,1)S(1)} %fusion.1.sh, bf16[2048,512]{1,0:T(8,128)(2,1)S(1)} %copy-done.1, bf16[1024,512]{1,0:T(8,128)(2,1)S(1)} %copy-done.2, bf16[256,512]{1,0:T(8,128)(2,1)S(1)} %copy-done), custom_call_target="tpu_custom_call" | custom-call | tf_op jit(solution)/shard_map/pallas_call | solution.py:605
  174.0 0.8 convert_multiply_fusion
  174.8 0.9 fusion.12
  175.7 0.8 fusion.13
  176.5 2.6 %convert_element_type.93 = f32[1,2048,512]{2,1,0:T(8,128)} convert(bf16[1,2048,512]{2,1,0:T(8,128)(2,1)S(1)} %copy-done.6) | non-fusion elementwise | flops 1048576 | bytes 6291456 | tf_op jit(solution)/shard_map/convert_element_type | solution.py:739
  179.1 2.6 %convert_element_type.94 = f32[1,2048,512]{2,1,0:T(8,128)} convert(bf16[1,2048,512]{2,1,0:T(8,128)(2,1)S(1)} %copy-done.5) | non-fusion elementwise | flops 1048576 | bytes 6291456 | tf_op jit(solution)/shard_map/convert_element_type | solution.py:740
  181.7 2.5 %convert_element_type.95 = f32[1,512,2048]{2,1,0:T(8,128)} convert(bf16[1,512,2048]{2,1,0:T(8,128)(2,1)S(1)} %copy-done.4) | non-fusion elementwise | flops 1048576 | bytes 6291456 | tf_op jit(solution)/shard_map/convert_element_type | solution.py:741
  184.3 0.7 copy.72
  (43 shorter events, 0.9 us)
Async XLA Ops:
  0.6 8.2 %copy-start.7 = (bf16[256,1024]{1,0:T(8,128)(2,1)S(1)}, bf16[256,1024]{1,0:T(8,128)(2,1)}, u32[]{:S(2)}) copy-start(bf16[256,1024]{1,0:T(8,128)(2,1)} %stream_in.1) | copy-start | bytes 1572868
  0.6 9.9 %copy-start.10 = (bf16[256,1024]{1,0:T(8,128)(2,1)S(1)}, bf16[256,1024]{1,0:T(8,128)(2,1)}, u32[]{:S(2)}) copy-start(bf16[256,1024]{1,0:T(8,128)(2,1)} %grad_in.1) | copy-start | bytes 1572868
  3.7 8.3 %copy-start.12 = (f32[3,512]{1,0:T(4,128)S(1)}, f32[3,512]{1,0:T(4,128)}, u32[]{:S(2)}) copy-start(f32[3,512]{1,0:T(4,128)} %param.17) | copy-start | bytes 18436
  3.7 8.3 %collective-permute-start.1 = (f32[4,256]{1,0:T(4,128)S(1)}, f32[4,256]{1,0:T(4,128)S(1)}, u32[]{:S(2)}, u32[]{:S(2)}) collective-permute-start(f32[4,256]{1,0:T(4,128)S(1)} %pad_maximum_fusion.2), channel_id=1, source_target_pairs={{0,16},{2,18},{4,20},{6,22},{8,24},{10,26},{12,28},{14,30},{16,0},... | collective-permute-start | bytes 12296 | tf_op jit(solution)/shard_map/ppermute | solution.py:681
  4.8 9.1 %copy-start = (bf16[256,512]{1,0:T(8,128)(2,1)S(1)}, bf16[256,512]{1,0:T(8,128)(2,1)}, u32[]{:S(2)}) copy-start(bf16[256,512]{1,0:T(8,128)(2,1)} %gate_in.1) | copy-start | bytes 786436
  4.8 9.1 %collective-permute-start = (f32[2,512]{1,0:T(2,128)S(1)}, f32[2,512]{1,0:T(2,128)S(1)}, u32[]{:S(2)}, u32[]{:S(2)}) collective-permute-start(f32[2,512]{1,0:T(2,128)S(1)} %slice.46), channel_id=1, source_target_pairs={{0,2},{2,4},{4,6},{6,8},{8,10},{10,12},{12,14},{14,16},{16,18},{18... | collective-permute-start | bytes 12296 | tf_op jit(solution)/shard_map/ppermute | solution.py:19
  14.8 126.5 %copy-start.11 = (bf16[256,1024]{1,0:T(8,128)(2,1)S(1)}, bf16[256,1024]{1,0:T(8,128)(2,1)}, u32[]{:S(2)}) copy-start(bf16[256,1024]{1,0:T(8,128)(2,1)} %grad_in.1) | copy-start | bytes 1572868
  141.3 2.1 %copy-start.1 = (bf16[2048,512]{1,0:T(8,128)(2,1)S(1)}, bf16[2048,512]{1,0:T(8,128)(2,1)}, u32[]{:S(2)}) copy-start(bf16[2048,512]{1,0:T(8,128)(2,1)} %w_out_hbm.1) | copy-start | bytes 6291460
  143.4 31.4 %copy-start.3 = (bf16[256,1024]{1,0:T(8,128)(2,1)}, bf16[256,1024]{1,0:T(8,128)(2,1)S(1)}, u32[]{:S(2)}) copy-start(bf16[256,1024]{1,0:T(8,128)(2,1)S(1)} %fusion.1.sh) | copy-start | bytes 1572868
  143.4 1.4 copy-start.2
  144.8 30.0 %copy-start.8 = (bf16[256,512]{1,0:T(8,128)(2,1)S(1)}, bf16[256,512]{1,0:T(8,128)(2,1)}, u32[]{:S(2)}) copy-start(bf16[256,512]{1,0:T(8,128)(2,1)} %param.15) | copy-start | bytes 786436
  174.0 1.8 copy-start.9
  174.0 2.5 %copy-start.6 = (bf16[1,2048,512]{2,1,0:T(8,128)(2,1)S(1)}, bf16[1,2048,512]{2,1,0:T(8,128)(2,1)}, u32[]{:S(2)}) copy-start(bf16[1,2048,512]{2,1,0:T(8,128)(2,1)} %get-tuple-element.23) | copy-start | bytes 6291460
  176.5 2.6 %copy-start.5 = (bf16[1,2048,512]{2,1,0:T(8,128)(2,1)S(1)}, bf16[1,2048,512]{2,1,0:T(8,128)(2,1)}, u32[]{:S(2)}) copy-start(bf16[1,2048,512]{2,1,0:T(8,128)(2,1)} %get-tuple-element.24) | copy-start | bytes 6291460
  179.1 2.6 %copy-start.4 = (bf16[1,512,2048]{2,1,0:T(8,128)(2,1)S(1)}, bf16[1,512,2048]{2,1,0:T(8,128)(2,1)}, u32[]{:S(2)}) copy-start(bf16[1,512,2048]{2,1,0:T(8,128)(2,1)} %get-tuple-element.25) | copy-start | bytes 6291460
where the time goes:
time: 188 us; the launch traced here: 185 us
  Pallas kernels  156 us (83%)
  other arithmetic  15.7 us (8%)
  matrix products  5.13 us (3%)
  local copies, waits for them, and re-layouts  4.31 us (2%)
  starting transfers between devices  3.31 us (2%)
    pallas_call x1, Pallas kernels, expert_pass(): pl.pallas_call(functools.partial(expert_kernel, count, cap), out_shape=(j...  126 us
    pallas_call x1, Pallas kernels, mixer_pass(): pl.pallas_call(functools.partial(mixer_kernel, count), out_shape=(jax.Sha...  29.2 us
    dot_general x4, matrix products, dot(): lax.dot_general(a, b, (((ca,), (cb,)), ((), ())), preferred_element_type=...  5.13 us
  transfers between devices with their start and end apart: 2, of which 0 were waited for; matrix products, arithmetic and copies ran while one was open for 4% of the time, Pallas kernels for 0%

commit v1 on v0

v1 whole, which is shorter than its diff:
```python
import functools

import jax
import jax.numpy as jnp
from jax import lax
from jax.experimental import pallas as pl
from jax.experimental.pallas import tpu as pltpu
from jax.sharding import PartitionSpec as P

MESH = pl.DeviceIdType.MESH
LAYERS = 4
PARTS = 4
CHUNKS = 4
F32 = jnp.float32
BF16 = jnp.bfloat16
OWN, NEXT, ACROSS, FAR = 0, 1, 2, 3


def passed_along(shard, axis, by):
    count = lax.axis_size(axis)
    pairs = [(i, i + by) for i in range(count) if 0 <= i + by < count]
    return lax.ppermute(shard, axis, pairs)


def dot(a, b, ca, cb):
    return lax.dot_general(a, b, (((ca,), (cb,)), ((), ())), preferred_element_type=F32)


def team_size(count):
    size = 1
    while size * size < count:
        size *= 2
    return size


def expert_kernel(
    count,
    cap,
    stream_in,
    grad_in,
    ids,
    weights,
    gate_in,
    conv_gate,
    conv_value,
    taps,
    wg_hbm,
    wu_hbm,
    wd_hbm,
    half_out,
    conv_out,
    mix_out,
    gate_out,
    up_out,
    down_out,
    toks_in,
    table,
    pick,
    scale,
    rel,
    rows,
    cot,
    wg,
    wu,
    wd,
    pre_g,
    pre_u,
    hidden,
    gg,
    ug,
    part_out,
    part_in,
    ret,
    back,
    col_out,
    col_in,
    total,
    gate_f,
    up_f,
    down_f,
    mix,
    mix_src,
    padded,
    halo_src,
    halo_dst,
    w_sem,
    out_sem,
    z_send,
    z_recv,
    t_send,
    t_recv,
    i_send,
    i_recv,
    f_send,
    f_recv,
    p_send,
    p_recv,
    r_send,
    r_recv,
    c_send,
    c_recv,
    m_send,
    m_recv,
    h_sem,
):
    me = lax.axis_index("sp")
    half = lax.axis_index("tp")
    other = 1 - half
    team = count // LAYERS
    place, layer = lax.rem(me, team), me // team
    side = layer // 2
    inner = lax.rem(layer + 1, LAYERS) >= 2
    outer = jnp.logical_not(inner)
    next_layer = layer + 1 - 2 * lax.rem(layer, 2)
    across_layer = 2 - side
    far_layer = 3 * (1 - side)
    toks, width = stream_in.shape
    slots = team * cap
    depth = taps.shape[0]
    top = ids.shape[0]

    def column(at):
        return (at * team + place, half)

    def teammate(i):
        return layer * team + lax.rem(place + i, team)

    loads = []
    for n, (a, b) in enumerate(((wg_hbm, wg), (wu_hbm, wu), (wd_hbm, wd))):
        load = pltpu.make_async_copy(a.at[0], b, w_sem.at[n])
        load.start()
        loads.append(load)

    after, before = lax.rem(me + 1, count), lax.rem(me + count - 1, count)
    barrier = pltpu.get_barrier_semaphore()

    def greet(device):
        pl.semaphore_signal(barrier, inc=1, device_id=device, device_id_type=MESH)

    greet(column(lax.rem(layer + 1, LAYERS)))
    greet(column(lax.rem(layer + 2, LAYERS)))
    greet(column(lax.rem(layer + 3, LAYERS)))

    @pl.loop(1, team)
    def _(i):
        greet((teammate(i), half))

    greet((me, other))
    greet((after, half))
    greet((before, half))
    pl.semaphore_wait(barrier, LAYERS - 1 + team - 1 + 3)

    def remote(src, dst, send, recv, device):
        return pltpu.make_async_remote_copy(
            src_ref=src,
            dst_ref=dst,
            send_sem=send,
            recv_sem=recv,
            device_id=device,
            device_id_type=MESH,
        )

    def block(k):
        return pl.ds(pl.multiple_of(k * cap, cap), cap)

    def piece(j, k):
        return pl.ds(pl.multiple_of(j * slots + k * cap, cap), cap)

    def group(j):
        return pl.ds(j * slots, slots)

    whole = (stream_in, grad_in)

    def blocks_of(which, j):
        return whole[which] if j == OWN else toks_in.at[which, j - 1]

    stretch = toks // CHUNKS

    def hop(which, n, j, to, lands, c):
        at = pl.ds(c * stretch, stretch)
        return remote(
            blocks_of(which, j).at[at],
            toks_in.at[which, lands - 1, at],
            z_send.at[which, n, c],
            z_recv.at[which, lands - 1, c],
            column(to),
        )

    def own_to_next(which, c):
        return hop(which, 0, OWN, next_layer, NEXT, c)

    def own_to_across(which, c):
        return hop(which, 1, OWN, across_layer, ACROSS, c)

    def next_to_across(which, c):
        return hop(which, 2, NEXT, across_layer, FAR, c)

    def across_to_next(which, c):
        return hop(which, 3, ACROSS, next_layer, ACROSS, c)

    def far_to_next(which, c):
        return hop(which, 4, FAR, next_layer, FAR, c)

    def arrived(which, j):
        for c in range(CHUNKS):
            hop(which, 0, j, next_layer, j, c).wait_recv()

    def begin(copy, which):
        for c in range(CHUNKS):
            copy(which, c).start()

    def relay(*steps):
        for c in range(CHUNKS):
            for which, j, copy in steps:
                hop(which, 0, j, next_layer, j, c).wait_recv()
                copy(which, c).start()

    last = pl.ds(toks - 8, 8)
    halo_src[...] = conv_gate[last].astype(F32) * conv_value[last].astype(F32)
    halo = remote(halo_src, halo_dst, h_sem.at[0], h_sem.at[1], (after, half))
    halo.start()
    begin(own_to_next, 0)

    @pl.when(inner)
    def _():
        begin(own_to_across, 0)

    expert = lax.broadcasted_iota(jnp.int32, (count, toks), 0)
    hits = [ids[k : k + 1] == expert for k in range(top)]
    named = functools.reduce(jnp.logical_or, hits)
    named = jnp.where(named, 1.0, 0.0).astype(BF16)
    early = lax.broadcasted_iota(jnp.int32, (toks, toks), 0)
    late = lax.broadcasted_iota(jnp.int32, (toks, toks), 1)
    earlier = jnp.where(early < late, 1.0, 0.0).astype(BF16)
    spots = dot(named, earlier, 1, 0) + (expert * cap).astype(F32)
    table[OWN] = jnp.zeros(table.shape[1:], F32)
    for k in range(top):
        table[OWN, k : k + 1] = jnp.sum(jnp.where(hits[k], spots, 0.0), axis=0, keepdims=True)
        table[OWN, top + k : top + k + 1] = weights[k : k + 1]

    seen_as = jnp.where(inner, ACROSS, FAR)

    def table_copy(n, to, lands):
        return remote(
            table.at[OWN], table.at[lands], t_send.at[n], t_recv.at[lands], column(to)
        )

    tables = (
        table_copy(0, next_layer, NEXT),
        table_copy(1, across_layer, seen_as),
        table_copy(2, far_layer, seen_as),
    )
    for copy in tables:
        copy.start()

    begin(own_to_next, 1)

    base = (layer * slots).astype(F32)

    def choose(j):
        spot = lax.broadcasted_iota(jnp.int32, (slots, toks), 0).astype(F32)
        found = [table[j, k : k + 1] - base == spot for k in range(top)]
        pick[j] = jnp.where(functools.reduce(jnp.logical_or, found), 1.0, 0.0).astype(BF16)
        scale[j] = sum(
            jnp.sum(
                jnp.where(found[k], table[j, top + k : top + k + 1], 0.0), axis=1, keepdims=True
            )
            for k in range(top)
        )

    bufs = (rows, cot)

    def in_copy(which, j, i):
        return remote(
            rel.at[which, j, block(lax.rem(place + i, team))],
            bufs[which].at[half, piece(j, place)],
            i_send.at[which, j, i],
            i_recv.at[which, j, i],
            (teammate(i), half),
        )

    def in_arrival(which, j, i):
        at = bufs[which].at[half, piece(j, lax.rem(place - i + team, team))]
        return remote(at, at, i_send.at[which, j, i], i_recv.at[which, j, i], (teammate(i), half))

    def pass_copy(which, j, i):
        at = bufs[which].at[half, piece(j, lax.rem(place - i + team, team))]
        return remote(at, at, f_send.at[which, j, i], f_recv.at[which, j, i], (me, other))

    def own_pass(which, j):
        return remote(
            rel.at[which, j, block(place)],
            bufs[which].at[half, piece(j, place)],
            f_send.at[which, j, 0],
            f_recv.at[which, j, 0],
            (me, other),
        )

    def deal(which, j):
        chosen = dot(pick[j], blocks_of(which, j)[...], 1, 0)
        if which == 1:
            chosen = scale[j] * chosen
        rel[which, j] = chosen.astype(BF16)

        @pl.loop(1, team)
        def _(i):
            in_copy(which, j, i).start()

        own_pass(which, j).start()
        bufs[which][half, piece(j, place)] = rel[which, j, block(place)]

    def gather(which, j):
        @pl.loop(1, team)
        def _(i):
            in_arrival(which, j, i).wait_recv()
            pass_copy(which, j, i).start()

        @pl.loop(0, team)
        def _(i):
            pass_copy(which, j, i).wait_recv()

    mine_at = pl.ds(pl.multiple_of(half * width, width), width)
    other_at = pl.ds(pl.multiple_of(other * width, width), width)

    def part_copy(j):
        return remote(
            part_out.at[group(j)], part_in.at[group(j)], p_send.at[j], p_recv.at[j], (me, other)
        )

    def ret_copy(j, i):
        return remote(
            ret.at[piece(j, lax.rem(place + i, team))],
            back.at[piece(j, place)],
            r_send.at[j, i],
            r_recv.at[j, i],
            (teammate(i), half),
        )

    def ret_arrival(j, i):
        at = back.at[piece(j, lax.rem(place - i + team, team))]
        return remote(at, at, r_send.at[j, i], r_recv.at[j, i], (teammate(i), half))

    def ahead(j):
        gather(0, j)
        at = group(j)
        left, right = rows[0, at], rows[1, at]
        pre_g[at] = dot(left, wg[:width], 1, 0) + dot(right, wg[width:], 1, 0)
        pre_u[at] = dot(left, wu[:width], 1, 0) + dot(right, wu[width:], 1, 0)

    def behind(j):
        gather(1, j)
        at = group(j)
        grad = dot(cot[0, at], wd[:, :width], 1, 1) + dot(cot[1, at], wd[:, width:], 1, 1)
        pg, pu = pre_g[at], pre_u[at]
        sig = jax.nn.sigmoid(pg)
        silu = pg * sig
        hidden[at] = (silu * pu).astype(BF16)
        ug_now = (grad * silu).astype(BF16)
        gg_now = (grad * pu * sig * (1.0 + pg * (1.0 - sig))).astype(BF16)
        ug[at] = ug_now
        gg[at] = gg_now
        far = dot(gg_now, wg[other_at], 1, 1) + dot(ug_now, wu[other_at], 1, 1)
        part_out[at] = far.astype(BF16)
        part_copy(j).start()
        near = dot(gg_now, wg[mine_at], 1, 1) + dot(ug_now, wu[mine_at], 1, 1)
        near = near.astype(BF16).astype(F32)
        part_copy(j).wait_recv()
        ret[at] = (near + part_in[at].astype(F32)).astype(BF16)

        @pl.loop(1, team)
        def _(i):
            ret_copy(j, i).start()

        back[piece(j, place)] = ret[piece(j, place)]

    def returned(j):
        @pl.loop(1, team)
        def _(i):
            ret_arrival(j, i).wait_recv()

    share = width // PARTS

    def cols(n):
        return pl.ds(n * share, share)

    def sum_copy(j, n):
        if j == NEXT:
            to, lands = next_layer, 0
        else:
            to = jnp.where(inner, across_layer, next_layer)
            lands = jnp.where(inner, j - 1, j + 1)
        return remote(
            col_out.at[j - 1, :, cols(n)],
            col_in.at[lands, :, cols(n)],
            c_send.at[j - 1, n],
            c_recv.at[lands, n],
            column(to),
        )

    def sum_arrival(lands, n):
        at = col_in.at[lands, :, cols(n)]
        return remote(at, at, c_send.at[0, n], c_recv.at[lands, n], column(next_layer))

    def partial(j, n):
        return dot(pick[j], back[group(j), cols(n)], 0, 0)

    def send_sums(j):
        for n in range(PARTS):
            col_out[j - 1, :, cols(n)] = partial(j, n).astype(BF16)
            sum_copy(j, n).start()

    def forward_sums(*js):
        for n in range(PARTS):
            for j in js:
                mine = partial(j, n)
                sum_arrival(j + 1, n).wait_recv()
                mine = mine + col_in[j + 1, :, cols(n)].astype(F32)
                col_out[j - 1, :, cols(n)] = mine.astype(BF16)
                sum_copy(j, n).start()

    choose(OWN)
    deal(0, OWN)
    deal(1, OWN)

    halo.wait_recv()
    prod = conv_gate[...].astype(F32) * conv_value[...].astype(F32)
    padded[8:] = prod
    padded[:8] = jnp.where(me == 0, 0.0, halo_dst[...])
    conv = jnp.zeros(prod.shape, F32)
    for tap in range(depth):
        start = 8 - (depth - 1) + tap
        conv = conv + taps[tap : tap + 1] * padded[start : start + toks]
    conv_out[...] = conv
    mix_src[...] = (gate_in[...].astype(F32) * conv).astype(BF16)

    crew = team_size(count)
    seat = lax.rem(me, crew)

    def mix_copy(j):
        return remote(
            mix_src,
            mix.at[pl.ds(pl.multiple_of(j * toks, toks), toks)],
            m_send.at[j],
            m_recv.at[j],
            (me - seat + lax.rem(seat + j, crew), half),
        )

    def informed(j):
        table_copy(0, next_layer, j).wait_recv()
        choose(j)

    @pl.when(inner)
    def _():
        relay((0, NEXT, next_to_across), (0, ACROSS, across_to_next))

    @pl.when(outer)
    def _():
        arrived(0, NEXT)

    informed(NEXT)
    deal(0, NEXT)
    for load in loads:
        load.wait()

    @pl.when(inner)
    def _():
        relay((1, NEXT, next_to_across), (0, FAR, far_to_next))
        begin(own_to_across, 1)

    @pl.when(outer)
    def _():
        arrived(1, NEXT)

    deal(1, NEXT)
    ahead(OWN)
    behind(OWN)

    @pl.when(inner)
    def _():
        relay((1, FAR, far_to_next))

    ahead(NEXT)
    behind(NEXT)

    @pl.when(outer)
    def _():
        arrived(0, ACROSS)

    informed(ACROSS)
    deal(0, ACROSS)
    returned(OWN)
    total[...] = dot(pick[OWN], back[group(OWN)], 0, 0)
    returned(NEXT)

    @pl.when(outer)
    def _():
        send_sums(NEXT)
        arrived(0, FAR)

    informed(FAR)
    deal(0, FAR)

    @pl.when(inner)
    def _():
        relay((1, ACROSS, across_to_next))

    ahead(ACROSS)

    @pl.when(outer)
    def _():
        arrived(1, FAR)

    deal(1, FAR)
    ahead(FAR)

    @pl.when(outer)
    def _():
        arrived(1, ACROSS)

    deal(1, ACROSS)
    behind(FAR)
    behind(ACROSS)

    @pl.loop(1, crew)
    def _(j):
        mix_copy(j).start()

    mix[pl.ds(0, toks)] = mix_src[...]
    returned(FAR)

    @pl.when(outer)
    def _():
        send_sums(FAR)

    hid_tile = min(256, hidden.shape[1])

    @pl.loop(0, hidden.shape[1] // hid_tile)
    def _(t):
        to = pl.ds(pl.multiple_of(t * hid_tile, hid_tile), hid_tile)
        x = hidden[:, to].T
        for h in range(2):
            down_f[to, h * width : (h + 1) * width] = dot(x, cot[h], 1, 0).astype(BF16)

    stores = [pltpu.make_async_copy(down_f, down_out.at[0], out_sem.at[2])]
    stores[-1].start()

    tile = 256
    per_half = width // tile

    @pl.loop(0, 2 * per_half)
    def _(t):
        h, c = t // per_half, lax.rem(t, per_half)
        at = pl.ds(pl.multiple_of(c * tile, tile), tile)
        to = pl.ds(pl.multiple_of(t * tile, tile), tile)
        x = rows[h, :, at].T
        gate_f[to] = dot(x, gg[...], 1, 0).astype(BF16)
        up_f[to] = dot(x, ug[...], 1, 0).astype(BF16)

    stores.append(pltpu.make_async_copy(gate_f, gate_out.at[0], out_sem.at[0]))
    stores.append(pltpu.make_async_copy(up_f, up_out.at[0], out_sem.at[1]))
    for store in stores[1:]:
        store.start()

    returned(ACROSS)

    @pl.when(outer)
    def _():
        send_sums(ACROSS)

    @pl.when(inner)
    def _():
        forward_sums(FAR)
        forward_sums(NEXT, ACROSS)

        for n in range(PARTS):
            sum_arrival(1, n).wait_recv()
            total[:, cols(n)] += col_in[1, :, cols(n)].astype(F32)

    for n in range(PARTS):
        sum_arrival(0, n).wait_recv()
        now = total[:, cols(n)] + col_in[0, :, cols(n)].astype(F32)
        half_out[:, cols(n)] = (grad_in[:, cols(n)].astype(F32) + now).astype(BF16)

    for which in range(2):
        for c in range(CHUNKS):
            own_to_next(which, c).wait_send()

        for j in range(LAYERS):
            own_pass(which, j).wait_send()

            @pl.loop(1, team)
            def _(i):
                in_copy(which, j, i).wait_send()
                pass_copy(which, j, i).wait_send()

    @pl.when(inner)
    def _():
        for which in range(2):
            for copy in (own_to_across, next_to_across, across_to_next, far_to_next):
                for c in range(CHUNKS):
                    copy(which, c).wait_send()

    for j in range(LAYERS):
        part_copy(j).wait_send()

        @pl.loop(1, team)
        def _(i):
            ret_copy(j, i).wait_send()

    for j in (NEXT, ACROSS, FAR):
        for n in range(PARTS):
            sum_copy(j, n).wait_send()

    for copy in tables:
        copy.wait_send()
    halo.wait_send()

    @pl.loop(1, crew)
    def _(j):
        mix_copy(j).wait_send()
        mix_copy(j).wait_recv()

    mix_out[...] = mix[...]
    for store in stores:
        store.wait()


def expert_pass(
    stream, out_grad, ids, weights, gate_in, conv_gate, conv_value, taps, w_gate, w_up, w_down
):
    toks, width = stream.shape
    chans = gate_in.shape[1]
    count = lax.axis_size("sp")
    cap = 4 * toks // count
    team = count // LAYERS
    slots = team * cap
    tall = LAYERS * slots
    deep, hid = w_gate.shape[1:]
    crew = team_size(count)
    vmem = pl.BlockSpec(memory_space=pltpu.VMEM)
    anywhere = pl.BlockSpec(memory_space=pl.ANY)
    dma = pltpu.SemaphoreType.DMA
    return pl.pallas_call(
        functools.partial(expert_kernel, count, cap),
        out_shape=(
            jax.ShapeDtypeStruct((toks, width), BF16),
            jax.ShapeDtypeStruct((toks, chans), F32),
            jax.ShapeDtypeStruct((crew * toks, chans), BF16),
            jax.ShapeDtypeStruct((1, deep, hid), BF16),
            jax.ShapeDtypeStruct((1, deep, hid), BF16),
            jax.ShapeDtypeStruct((1, hid, deep), BF16),
        ),
        in_specs=[vmem] * 8 + [anywhere] * 3,
        out_specs=(vmem, vmem, vmem, anywhere, anywhere, anywhere),
        scratch_shapes=[
            pltpu.VMEM((2, LAYERS - 1, toks, width), BF16),
            pltpu.VMEM((LAYERS, 8, toks), F32),
            pltpu.VMEM((LAYERS, slots, toks), BF16),
            pltpu.VMEM((LAYERS, slots, 1), F32),
            pltpu.VMEM((2, LAYERS, slots, width), BF16),
            pltpu.VMEM((2, tall, width), BF16),
            pltpu.VMEM((2, tall, width), BF16),
            pltpu.VMEM((deep, hid), BF16),
            pltpu.VMEM((deep, hid), BF16),
            pltpu.VMEM((hid, deep), BF16),
            pltpu.VMEM((tall, hid), F32),
            pltpu.VMEM((tall, hid), F32),
            pltpu.VMEM((tall, hid), BF16),
            pltpu.VMEM((tall, hid), BF16),
            pltpu.VMEM((tall, hid), BF16),
            pltpu.VMEM((tall, width), BF16),
            pltpu.VMEM((tall, width), BF16),
            pltpu.VMEM((tall, width), BF16),
            pltpu.VMEM((tall, width), BF16),
            pltpu.VMEM((LAYERS - 1, toks, width), BF16),
            pltpu.VMEM((5, toks, width), BF16),
            pltpu.VMEM((toks, width), F32),
            pltpu.VMEM((deep, hid), BF16),
            pltpu.VMEM((deep, hid), BF16),
            pltpu.VMEM((hid, deep), BF16),
            pltpu.VMEM((crew * toks, chans), BF16),
            pltpu.VMEM((toks, chans), BF16),
            pltpu.VMEM((toks + 8, chans), F32),
            pltpu.VMEM((8, chans), F32),
            pltpu.VMEM((8, chans), F32),
            dma((3,)),
            dma((3,)),
            dma((2, 5, CHUNKS)),
            dma((2, LAYERS - 1, CHUNKS)),
            dma((3,)),
            dma((LAYERS,)),
            dma((2, LAYERS, team)),
            dma((2, LAYERS, team)),
            dma((2, LAYERS, team)),
            dma((2, LAYERS, team)),
            dma((LAYERS,)),
            dma((LAYERS,)),
            dma((LAYERS, team)),
            dma((LAYERS, team)),
            dma((LAYERS - 1, PARTS)),
            dma((5, PARTS)),
            dma((crew,)),
            dma((crew,)),
            dma((2,)),
        ],
        compiler_params=pltpu.CompilerParams(
            collective_id=0, has_side_effects=True, vmem_limit_bytes=62 * 1024 * 1024
        ),
    )(stream, out_grad, ids, weights, gate_in, conv_gate, conv_value, taps, w_gate, w_up, w_down)


def mixer_kernel(
    count,
    sh,
    w_out_hbm,
    mix,
    gate_in,
    wog_out,
    mg_out,
    halo_out,
    far,
    w_out,
    sg,
    p_send,
    p_recv,
    h_send,
    h_recv,
    w_sem,
    whole_sem,
    gsend_sem,
    grecv_sem,
    fsend_sem,
    frecv_sem,
    own_sem,
    psend_sem,
    precv_sem,
    hsem,
):
    me = lax.axis_index("sp")
    half = lax.axis_index("tp")
    other = 1 - half
    team = team_size(count)
    layers = count // team
    place, layer = lax.rem(me, team), me // team
    toks, width = sh.shape
    per = layers // 2
    blk = width // (team * per)
    load = pltpu.make_async_copy(w_out_hbm, w_out, w_sem)
    load.start()

    def member(j):
        return me - place + lax.rem(place + j, team)

    def floor(i):
        return lax.rem(layer + i, layers) * team + place

    after, before = lax.rem(me + 1, count), lax.rem(me + count - 1, count)
    barrier = pltpu.get_barrier_semaphore()

    def greet(device):
        pl.semaphore_signal(barrier, inc=1, device_id=device, device_id_type=MESH)

    for j in range(1, team):
        greet((member(j), half))
    for i in range(1, layers):
        greet((floor(i), half))
    greet((me, other))
    greet((after, half))
    greet((before, half))
    pl.semaphore_wait(barrier, team - 1 + layers - 1 + 3)

    def remote(src, dst, send, recv, device):
        return pltpu.make_async_remote_copy(
            src_ref=src,
            dst_ref=dst,
            send_sem=send,
            recv_sem=recv,
            device_id=device,
            device_id_type=MESH,
        )

    def cols(j, m):
        at = (lax.rem(place + j, team) + team * m) * blk
        return pl.ds(pl.multiple_of(at, blk), blk)

    def spot(h, m, size):
        return pl.ds(pl.multiple_of((h * per + m) * blk, blk), size)

    def stripe(j):
        return pl.ds(j * toks, toks)

    def piece(j, m):
        return remote(
            sh.at[:, cols(j, m)],
            sg.at[stripe(j), spot(half, m, blk)],
            gsend_sem.at[j, m],
            grecv_sem.at[j, m],
            (member(j), half),
        )

    def own_piece(m):
        return remote(
            sh.at[:, cols(0, m)],
            sg.at[stripe(0), spot(half, m, blk)],
            own_sem.at[0, m],
            own_sem.at[1, m],
            (me, other),
        )

    def handed(j):
        ref = sg.at[stripe(j), spot(half, 0, per * blk)]
        return remote(ref, ref, fsend_sem.at[j], frecv_sem.at[j], (me, other))

    whole = remote(sh, far, whole_sem.at[0], whole_sem.at[1], (me, other))
    whole.start()
    for j in range(1, team):
        for m in range(per):
            piece(j, m).start()
    for m in range(per):
        own_piece(m).start()
        sg[stripe(0), spot(half, m, blk)] = sh[:, cols(0, m)]

    load.wait()
    near_at = pl.ds(pl.multiple_of(half * width, width), width)
    far_at = pl.ds(pl.multiple_of(other * width, width), width)
    grad = dot(sh[...], w_out[near_at], 1, 0)
    whole.wait_recv()
    grad = (grad + dot(far[...], w_out[far_at], 1, 0)).astype(BF16)
    mg_out[...] = grad
    h_send[...] = grad[:8].astype(F32) * gate_in[:8].astype(F32)
    halo = remote(h_send, h_recv, hsem.at[0], hsem.at[1], (before, half))
    halo.start()
    for j in range(1, team):
        for m in range(per):
            piece(j, m).wait_recv()
        handed(j).start()
    for m in range(per):
        own_piece(m).wait_recv()
    for j in range(1, team):
        handed(j).wait_recv()

    def share(i):
        at = pl.ds(pl.multiple_of(lax.rem(layer + i, layers) * blk, blk), blk)
        return dot(sg[:, at].T, mix[...], 1, 0)

    def part(i):
        return remote(
            p_send.at[i], p_recv.at[i], psend_sem.at[i], precv_sem.at[i], (floor(i), half)
        )

    @pl.loop(1, layers)
    def _(i):
        p_send[i] = share(i).astype(BF16)
        part(i).start()

    wog_out[...] = share(0)
    for m in range(per):
        own_piece(m).wait_send()
    whole.wait_send()
    for j in range(1, team):
        for m in range(per):
            piece(j, m).wait_send()
        handed(j).wait_send()
    halo.wait_send()
    halo.wait_recv()
    halo_out[...] = h_recv[...]

    @pl.loop(1, layers)
    def _(i):
        part(i).wait_recv()
        wog_out[...] += p_recv[i].astype(F32)

    @pl.loop(1, layers)
    def _(i):
        part(i).wait_send()


def mixer_pass(stream_half, w_out, mix, gate_in):
    count = lax.axis_size("sp")
    team = team_size(count)
    layers = count // team
    per = layers // 2
    toks, width = stream_half.shape
    deep, chans = w_out.shape
    blk = deep // count
    vmem = pl.BlockSpec(memory_space=pltpu.VMEM)
    dma = pltpu.SemaphoreType.DMA
    return pl.pallas_call(
        functools.partial(mixer_kernel, count),
        out_shape=(
            jax.ShapeDtypeStruct((blk, chans), F32),
            jax.ShapeDtypeStruct((toks, chans), BF16),
            jax.ShapeDtypeStruct((8, chans), F32),
        ),
        in_specs=[vmem, pl.BlockSpec(memory_space=pl.ANY), vmem, vmem],
        out_specs=(vmem, vmem, vmem),
        scratch_shapes=[
            pltpu.VMEM((toks, width), BF16),
            pltpu.VMEM((deep, chans), BF16),
            pltpu.VMEM((team * toks, layers * blk), BF16),
            pltpu.VMEM((layers, blk, chans), BF16),
            pltpu.VMEM((layers, blk, chans), BF16),
            pltpu.VMEM((8, chans), F32),
            pltpu.VMEM((8, chans), F32),
            dma,
            dma((2,)),
            dma((team, per)),
            dma((team, per)),
            dma((team,)),
            dma((team,)),
            dma((2, per)),
            dma((layers,)),
            dma((layers,)),
            dma((2,)),
        ],
        compiler_params=pltpu.CompilerParams(
            collective_id=1, has_side_effects=True, vmem_limit_bytes=32 * 1024 * 1024
        ),
    )(stream_half, w_out, mix, gate_in)


def shards(
    stream,
    out_grad,
    gate_in,
    conv_gate,
    conv_value,
    taps,
    w_out,
    route_ids,
    route_weights,
    w_gate,
    w_up,
    w_down,
):
    tok_rows = stream.shape[0]
    me = lax.axis_index("sp")
    depth = taps.shape[0]
    channels = conv_gate.shape[1]
    stream_half, conv_sum, mix, gate_w_grad, up_w_grad, down_w_grad = expert_pass(
        stream,
        out_grad,
        route_ids.T,
        route_weights.T,
        gate_in,
        conv_gate,
        conv_value,
        taps,
        w_gate,
        w_up,
        w_down,
    )
    if w_out.shape[0] // lax.axis_size("sp") % 128 == 0:
        out_proj_grad, mixer_grad, halo = mixer_pass(stream_half, w_out, mix, gate_in)
    else:
        stream_whole = lax.all_gather(stream_half, "tp", axis=1, tiled=True)
        mixer_grad = dot(stream_whole, w_out, 1, 0).astype(BF16)
        out_proj_grad = lax.psum_scatter(
            dot(stream_whole, mix[:tok_rows], 0, 0).astype(BF16), "sp", scatter_dimension=0, tiled=True
        ).astype(F32)
        first = mixer_grad[: depth - 1].astype(F32) * gate_in[: depth - 1].astype(F32)
        halo = passed_along(first, "sp", -1)
    mixer_wide = mixer_grad.astype(jnp.float32)
    gate_in_grad = (mixer_wide * conv_sum).astype(jnp.bfloat16)
    conv_inner = mixer_wide * gate_in.astype(jnp.float32)
    right_rows = jnp.where(me == lax.axis_size("sp") - 1, 0.0, halo[: depth - 1])
    padded_back = jnp.concatenate([conv_inner, right_rows], axis=0)
    prod_grad = jnp.zeros((tok_rows, channels), jnp.float32)
    for tap_index in range(depth):
        offset = depth - 1 - tap_index
        prod_grad = prod_grad + taps[tap_index][None, :] * padded_back[offset : offset + tok_rows]
    conv_gate_grad = (prod_grad * conv_value.astype(jnp.float32)).astype(jnp.bfloat16)
    conv_value_grad = (prod_grad * conv_gate.astype(jnp.float32)).astype(jnp.bfloat16)
    return (
        stream_half,
        gate_in_grad,
        conv_gate_grad,
        conv_value_grad,
        out_proj_grad,
        gate_w_grad.astype(F32),
        up_w_grad.astype(F32),
        down_w_grad.astype(F32),
    )


def solution(mesh):
    placed = (
        P("sp", "tp"),
        P("sp", "tp"),
        P("sp", "tp"),
        P("sp", "tp"),
        P("sp", "tp"),
        P(None, "tp"),
        P(None, "tp"),
        P("sp", None),
        P("sp", None),
        P("sp", None, "tp"),
        P("sp", None, "tp"),
        P("sp", "tp", None),
    )
    return jax.shard_map(
        shards,
        mesh=mesh,
        in_specs=placed,
        out_specs=(
            P("sp", "tp"),
            P("sp", "tp"),
            P("sp", "tp"),
            P("sp", "tp"),
            P("sp", "tp"),
            P("sp", None, "tp"),
            P("sp", None, "tp"),
            P("sp", "tp", None),
        ),
        check_vma=False,
    )
```

time: 188 us -> 166 us (0.88)
  Pallas kernels: 156 us -> 147 us
  other arithmetic: 15.7 us -> 10.3 us
  matrix products: 5.13 us -> 0 us
  starting transfers between devices: 3.31 us -> 0 us
  local copies, waits for them, and re-layouts: 4.31 us -> 6.19 us
    pallas_call x1, Pallas kernels: 126 us -> 115 us  [expert_pass(): pl.pallas_call(functools.partial(expert_kernel, count, cap), out_shape=(j...]
    dot_general x4 -> x0, matrix products: 5.13 us -> none  [dot(): lax.dot_general(a, b, (((ca,), (cb,)), ((), ())), preferred_element_type=...]
    ppermute x2 -> x0, starting transfers between devices: 3.31 us -> none  [the longest x1 3.25 us: passed_along(): return lax.ppermute(shard, axis, pairs)]
    unnamed x27 -> x22, local copies, waits for them, and re-layouts: 2.17 us -> 5.37 us
    pallas_call x1, Pallas kernels: 29.2 us -> 31.8 us  [mixer_pass(): pl.pallas_call(functools.partial(mixer_kernel, count), out_shape=(jax.Sha...]
    convert_element_type x5 -> x0, other arithmetic: 2.44 us -> none  [the longest x1 0.91 us: shards(): mixer_out = (gate_in.astype(jnp.float32) * conv_sum).astype(jnp.bfloat16)]
  transfers between devices with their start and end apart: 2 -> 0, of which waited for: 0 -> 0; matrix products, arithmetic and copies ran while one was open for 4% -> 0% of each run, Pallas kernels for 0% -> 0%
where the time goes in v1:
time: 166 us; the launch traced here: 164 us
  Pallas kernels  147 us (89%)
  other arithmetic  10.3 us (6%)
  local copies, waits for them, and re-layouts  6.19 us (4%)
    pallas_call x1, Pallas kernels, expert_pass(): pl.pallas_call(functools.partial(expert_kernel, count, cap), out_shape=(j...  115 us
    pallas_call x1, Pallas kernels, mixer_pass(): pl.pallas_call(functools.partial(mixer_kernel, count), out_shape=(jax.Sha...  31.8 us
    unnamed x22, local copies, waits for them, and re-layouts  5.37 us

profile of v1, /device:TPU:29, one launch (start us, length us, event | category | flops | bytes accessed | tf_op | source)
XLA Modules:
  0.0 164.1 jit_solution(12689457237404292386)
XLA Ops:
  0.6 0.8 fusion.7
  1.5 115.2 %shard_map.179 = (bf16[256,1024]{1,0:T(8,128)(2,1)}, f32[256,512]{1,0:T(8,128)}, bf16[1024,512]{1,0:T(8,128)(2,1)}, bf16[1,2048,512]{2,1,0:T(8,128)(2,1)}, bf16[...) custom-call(bf16[256,1024]{1,0:T(8,128)(2,1)} %stream_in.1, bf16[256,1024]{1,0:T(8,128)(2,1)} %grad_in.1, ...), custom_call_target="tpu_custom_call" | custom-call | tf_op jit(solution)/shard_map/pallas_call | solution.py:643
  116.6 0.0 copy-done
  116.7 0.0 copy-start.1
  116.7 1.0 copy-done.1
  117.7 1.6 copy-done.2
  119.3 1.2 copy-done.3
  120.5 31.8 %shard_map.180 = (f32[128,512]{1,0:T(8,128)S(1)}, bf16[256,512]{1,0:T(8,128)(2,1)S(1)}, f32[8,512]{1,0:T(8,128)S(1)}) custom-call(bf16[256,1024]{1,0:T(8,128)(2,1)S(1)} %copy-done.1, bf16[2048,512]{1,0:T(8,128)(2,1)S(1)} %copy-done.2, bf16[1024,512]{1,0:T(8,128)(2,1)S(1)} %copy-done.3, bf16[256,512]{1,0:T(8,128)(2,1)S(1)} %copy-done), custom_call_target="tpu_custom_call" | custom-call | tf_op jit(solution)/shard_map/pallas_call | solution.py:888
  152.3 0.0 copy-start.8
  152.3 0.0 copy-done.9
  152.3 0.0 copy-start.6
  152.3 0.8 convert_multiply_fusion
  153.1 0.0 copy-done.7
  153.1 0.9 multiply_convert_fusion
  154.1 0.0 copy-done.8
  154.1 0.8 multiply_convert_fusion.1
  154.8 0.0 copy-done.6
  154.8 2.6 %convert_element_type.37 = f32[1,2048,512]{2,1,0:T(8,128)} convert(bf16[1,2048,512]{2,1,0:T(8,128)(2,1)S(1)} %copy-done.6) | non-fusion elementwise | flops 1048576 | bytes 6291456 | tf_op jit(solution)/shard_map/convert_element_type | solution.py:980
  157.4 0.0 copy-done.5
  157.4 2.6 %convert_element_type.38 = f32[1,2048,512]{2,1,0:T(8,128)} convert(bf16[1,2048,512]{2,1,0:T(8,128)(2,1)S(1)} %copy-done.5) | non-fusion elementwise | flops 1048576 | bytes 6291456 | tf_op jit(solution)/shard_map/convert_element_type | solution.py:981
  160.1 0.0 copy-done.4
  160.1 2.5 %convert_element_type.39 = f32[1,512,2048]{2,1,0:T(8,128)} convert(bf16[1,512,2048]{2,1,0:T(8,128)(2,1)S(1)} %copy-done.4) | non-fusion elementwise | flops 1048576 | bytes 6291456 | tf_op jit(solution)/shard_map/convert_element_type | solution.py:982
  162.6 0.8 copy.22
  163.4 0.7 copy.23
  (8 shorter events, 0.0 us)
Async XLA Ops:
  1.5 115.2 %copy-start = (bf16[256,512]{1,0:T(8,128)(2,1)S(1)}, bf16[256,512]{1,0:T(8,128)(2,1)}, u32[]{:S(2)}) copy-start(bf16[256,512]{1,0:T(8,128)(2,1)} %gate_in.3) | copy-start | bytes 786436
  116.7 1.0 copy-start.1
  117.7 1.6 copy-start.2
  119.3 1.2 copy-start.3
  120.5 31.8 %copy-start.9 = (f32[256,512]{1,0:T(8,128)S(1)}, f32[256,512]{1,0:T(8,128)}, u32[]{:S(2)}) copy-start(f32[256,512]{1,0:T(8,128)} %get-tuple-element.20) | copy-start | bytes 1572868
  120.5 32.6 %copy-start.7 = (bf16[256,512]{1,0:T(8,128)(2,1)S(1)}, bf16[256,512]{1,0:T(8,128)(2,1)}, u32[]{:S(2)}) copy-start(bf16[256,512]{1,0:T(8,128)(2,1)} %conv_gate.1) | copy-start | bytes 786436
  152.3 1.8 %copy-start.8 = (bf16[256,512]{1,0:T(8,128)(2,1)S(1)}, bf16[256,512]{1,0:T(8,128)(2,1)}, u32[]{:S(2)}) copy-start(bf16[256,512]{1,0:T(8,128)(2,1)} %conv_value.1) | copy-start | bytes 786436
  152.3 2.5 %copy-start.6 = (bf16[1,2048,512]{2,1,0:T(8,128)(2,1)S(1)}, bf16[1,2048,512]{2,1,0:T(8,128)(2,1)}, u32[]{:S(2)}) copy-start(bf16[1,2048,512]{2,1,0:T(8,128)(2,1)} %get-tuple-element.23) | copy-start | bytes 6291460
  154.8 2.6 %copy-start.5 = (bf16[1,2048,512]{2,1,0:T(8,128)(2,1)S(1)}, bf16[1,2048,512]{2,1,0:T(8,128)(2,1)}, u32[]{:S(2)}) copy-start(bf16[1,2048,512]{2,1,0:T(8,128)(2,1)} %get-tuple-element.24) | copy-start | bytes 6291460
  157.4 2.6 %copy-start.4 = (bf16[1,512,2048]{2,1,0:T(8,128)(2,1)S(1)}, bf16[1,512,2048]{2,1,0:T(8,128)(2,1)}, u32[]{:S(2)}) copy-start(bf16[1,512,2048]{2,1,0:T(8,128)(2,1)} %get-tuple-element.25) | copy-start | bytes 6291460

commit v2 on v1

--- a/solution.py
+++ b/solution.py
@@ -26,16 +26,10 @@
     return lax.dot_general(a, b, (((ca,), (cb,)), ((), ())), preferred_element_type=F32)
 
 
-def team_size(count):
-    size = 1
-    while size * size < count:
-        size *= 2
-    return size
-
-
 def expert_kernel(
     count,
     cap,
+    fused,
     stream_in,
     grad_in,
     ids,
@@ -47,12 +41,15 @@
     wg_hbm,
     wu_hbm,
     wd_hbm,
+    wo_hbm,
     half_out,
-    conv_out,
-    mix_out,
     gate_out,
     up_out,
     down_out,
+    first_out,
+    second_out,
+    third_out,
+    fourth_out,
     toks_in,
     table,
     pick,
@@ -81,8 +78,16 @@
     mix,
     mix_src,
     padded,
+    conv_sum,
     halo_src,
     halo_dst,
+    wo,
+    far_half,
+    strips,
+    share_out,
+    share_in,
+    edge_src,
+    edge_dst,
     w_sem,
     out_sem,
     z_send,
@@ -102,6 +107,16 @@
     m_send,
     m_recv,
     h_sem,
+    g_send,
+    g_recv,
+    own_sem,
+    d_send,
+    d_recv,
+    s_send,
+    s_recv,
+    b_send,
+    b_recv,
+    e_sem,
 ):
     me = lax.axis_index("sp")
     half = lax.axis_index("tp")
@@ -128,6 +143,10 @@
     loads = []
     for n, (a, b) in enumerate(((wg_hbm, wg), (wu_hbm, wu), (wd_hbm, wd))):
         load = pltpu.make_async_copy(a.at[0], b, w_sem.at[n])
+        load.start()
+        loads.append(load)
+    if fused:
+        load = pltpu.make_async_copy(wo_hbm, wo, w_sem.at[3])
         load.start()
         loads.append(load)
 
@@ -409,14 +428,12 @@
             col_out[j - 1, :, cols(n)] = partial(j, n).astype(BF16)
             sum_copy(j, n).start()
 
-    def forward_sums(*js):
-        for n in range(PARTS):
-            for j in js:
-                mine = partial(j, n)
-                sum_arrival(j + 1, n).wait_recv()
-                mine = mine + col_in[j + 1, :, cols(n)].astype(F32)
-                col_out[j - 1, :, cols(n)] = mine.astype(BF16)
-                sum_copy(j, n).start()
+    def forward_sum(j, n):
+        mine = partial(j, n)
+        sum_arrival(j + 1, n).wait_recv()
+        mine = mine + col_in[j + 1, :, cols(n)].astype(F32)
+        col_out[j - 1, :, cols(n)] = mine.astype(BF16)
+        sum_copy(j, n).start()
 
     choose(OWN)
     deal(0, OWN)
@@ -430,11 +447,8 @@
     for tap in range(depth):
         start = 8 - (depth - 1) + tap
         conv = conv + taps[tap : tap + 1] * padded[start : start + toks]
-    conv_out[...] = conv
+    conv_sum[...] = conv
     mix_src[...] = (gate_in[...].astype(F32) * conv).astype(BF16)
-
-    crew = team_size(count)
-    seat = lax.rem(me, crew)
 
     def mix_copy(j):
         return remote(
@@ -442,7 +456,7 @@
             mix.at[pl.ds(pl.multiple_of(j * toks, toks), toks)],
             m_send.at[j],
             m_recv.at[j],
-            (me - seat + lax.rem(seat + j, crew), half),
+            (teammate(j), half),
         )
 
     def informed(j):
@@ -521,44 +535,50 @@
     behind(FAR)
     behind(ACROSS)
 
-    @pl.loop(1, crew)
-    def _(j):
-        mix_copy(j).start()
-
-    mix[pl.ds(0, toks)] = mix_src[...]
+    if fused:
+
+        @pl.loop(1, team)
+        def _(j):
+            mix_copy(j).start()
+
+        mix[pl.ds(0, toks)] = mix_src[...]
+
     returned(FAR)
 
     @pl.when(outer)
     def _():
         send_sums(FAR)
 
-    hid_tile = min(256, hidden.shape[1])
-
-    @pl.loop(0, hidden.shape[1] // hid_tile)
-    def _(t):
-        to = pl.ds(pl.multiple_of(t * hid_tile, hid_tile), hid_tile)
+    hid_part = hidden.shape[1] // PARTS
+    deep_part = width // PARTS
+
+    def weights_part(n):
+        to = pl.ds(n * hid_part, hid_part)
         x = hidden[:, to].T
         for h in range(2):
             down_f[to, h * width : (h + 1) * width] = dot(x, cot[h], 1, 0).astype(BF16)
 
-    stores = [pltpu.make_async_copy(down_f, down_out.at[0], out_sem.at[2])]
-    stores[-1].start()
-
-    tile = 256
-    per_half = width // tile
-
-    @pl.loop(0, 2 * per_half)
-    def _(t):
-        h, c = t // per_half, lax.rem(t, per_half)
-        at = pl.ds(pl.multiple_of(c * tile, tile), tile)
-        to = pl.ds(pl.multiple_of(t * tile, tile), tile)
-        x = rows[h, :, at].T
-        gate_f[to] = dot(x, gg[...], 1, 0).astype(BF16)
-        up_f[to] = dot(x, ug[...], 1, 0).astype(BF16)
-
-    stores.append(pltpu.make_async_copy(gate_f, gate_out.at[0], out_sem.at[0]))
-    stores.append(pltpu.make_async_copy(up_f, up_out.at[0], out_sem.at[1]))
-    for store in stores[1:]:
+        @pl.loop(0, 2)
+        def _(h):
+            to = pl.ds(pl.multiple_of(h * width + n * deep_part, deep_part), deep_part)
+            x = rows[h, :, n * deep_part : (n + 1) * deep_part].T
+            gate_f[to] = dot(x, gg[...], 1, 0).astype(BF16)
+            up_f[to] = dot(x, ug[...], 1, 0).astype(BF16)
+
+    for n in range(PARTS):
+
+        @pl.when(inner)
+        def _():
+            forward_sum(FAR, n)
+
+        weights_part(n)
+
+    stores = [
+        pltpu.make_async_copy(gate_f, gate_out.at[0], out_sem.at[0]),
+        pltpu.make_async_copy(up_f, up_out.at[0], out_sem.at[1]),
+        pltpu.make_async_copy(down_f, down_out.at[0], out_sem.at[2]),
+    ]
+    for store in stores:
         store.start()
 
     returned(ACROSS)
@@ -569,17 +589,143 @@
 
     @pl.when(inner)
     def _():
-        forward_sums(FAR)
-        forward_sums(NEXT, ACROSS)
+        for n in range(PARTS):
+            forward_sum(NEXT, n)
+            forward_sum(ACROSS, n)
 
         for n in range(PARTS):
             sum_arrival(1, n).wait_recv()
             total[:, cols(n)] += col_in[1, :, cols(n)].astype(F32)
 
-    for n in range(PARTS):
+    per = LAYERS // 2
+    blk = width // (team * per)
+
+    def band(b):
+        return pl.ds(b * blk, blk)
+
+    def spot(h, m, size):
+        return pl.ds(pl.multiple_of((h * per + m) * blk, blk), size)
+
+    def stripe(j):
+        return pl.ds(pl.multiple_of(j * toks, toks), toks)
+
+    def piece_copy(b, j, m):
+        return remote(
+            half_out.at[:, band(b)],
+            strips.at[stripe(j), spot(half, m, blk)],
+            g_send.at[j, m],
+            g_recv.at[j, m],
+            (teammate(j), half),
+        )
+
+    def own_piece(b, m):
+        return remote(
+            half_out.at[:, band(b)],
+            strips.at[stripe(0), spot(half, m, blk)],
+            own_sem.at[0, m],
+            own_sem.at[1, m],
+            (me, other),
+        )
+
+    def whole_copy(n):
+        return remote(
+            half_out.at[:, cols(n)], far_half.at[:, cols(n)], b_send.at[n], b_recv.at[n], (me, other)
+        )
+
+    def handed(j):
+        at = strips.at[stripe(j), spot(half, 0, per * blk)]
+        return remote(at, at, d_send.at[j], d_recv.at[j], (me, other))
+
+    def layer_copy(i):
+        to = lax.rem(layer + i, LAYERS)
+        return remote(share_out.at[i], share_in.at[i], s_send.at[i], s_recv.at[i], column(to))
+
+    def settle(n):
         sum_arrival(0, n).wait_recv()
         now = total[:, cols(n)] + col_in[0, :, cols(n)].astype(F32)
         half_out[:, cols(n)] = (grad_in[:, cols(n)].astype(F32) + now).astype(BF16)
+        if fused:
+            whole_copy(n).start()
+            for b in range(n * share // blk, (n + 1) * share // blk):
+                j, m = lax.rem(b % team - place + team, team), b // team
+
+                @pl.when(j > 0)
+                def _():
+                    piece_copy(b, j, m).start()
+
+                @pl.when(j == 0)
+                def _():
+                    own_piece(b, m).start()
+                    strips[stripe(0), spot(half, m, blk)] = half_out[:, band(b)]
+
+    def edge_copy():
+        return remote(edge_src, edge_dst, e_sem.at[0], e_sem.at[1], (before, half))
+
+    def mixer_grad():
+        mixed = dot(half_out[...], wo[mine_at], 1, 0)
+        for n in range(PARTS):
+            whole_copy(n).wait_recv()
+        mixed = (mixed + dot(far_half[...], wo[other_at], 1, 0)).astype(BF16)
+        wide = mixed.astype(F32)
+        inner_conv = wide * gate_in[...].astype(F32)
+        edge_src[...] = inner_conv[:8]
+        edge_copy().start()
+        padded[:toks] = inner_conv
+        second_out[...] = (wide * conv_sum[...]).astype(BF16)
+
+    def conv_grads():
+        edge_copy().wait_recv()
+        padded[toks:] = jnp.where(me == count - 1, 0.0, edge_dst[...])
+        prod_grad = jnp.zeros((toks, taps.shape[1]), F32)
+        for tap in range(depth):
+            start = depth - 1 - tap
+            prod_grad = prod_grad + taps[tap : tap + 1] * padded[start : start + toks]
+        third_out[...] = (prod_grad * conv_value[...].astype(F32)).astype(BF16)
+        fourth_out[...] = (prod_grad * conv_gate[...].astype(F32)).astype(BF16)
+
+    def strips_in():
+        @pl.loop(1, team)
+        def _(j):
+            for m in range(per):
+                piece_copy(0, j, m).wait_recv()
+            handed(j).start()
+
+        for m in range(per):
+            own_piece(0, m).wait_recv()
+
+        @pl.loop(1, team)
+        def _(j):
+            handed(j).wait_recv()
+            mix_copy(j).wait_recv()
+
+    def layer_share(i):
+        at = pl.ds(pl.multiple_of(lax.rem(layer + i, LAYERS) * blk, blk), blk)
+        return dot(strips[:, at].T, mix[...], 1, 0)
+
+    def shares_out():
+        for i in (2, 1, 3):
+            share_out[i] = layer_share(i).astype(BF16)
+            layer_copy(i).start()
+        first_out[...] = layer_share(0)
+
+    def shares_in():
+        for i in (1, 3, 2):
+            layer_copy(i).wait_recv()
+            first_out[...] += share_in[i].astype(F32)
+
+    for n in range(PARTS):
+        settle(n)
+    if fused:
+        strips_in()
+        shares_out()
+        mixer_grad()
+        conv_grads()
+        shares_in()
+    else:
+        first_out[...] = conv_sum[...]
+        second_out[...] = mix_src[...]
+        fourth_out[...] = jnp.zeros(fourth_out.shape, fourth_out.dtype)
+        third_out[...] = jnp.zeros(third_out.shape, third_out.dtype)
 
     for which in range(2):
         for c in range(CHUNKS):
@@ -615,18 +761,41 @@
         copy.wait_send()
     halo.wait_send()
 
-    @pl.loop(1, crew)
-    def _(j):
-        mix_copy(j).wait_send()
-        mix_copy(j).wait_recv()
-
-    mix_out[...] = mix[...]
+    if fused:
+        edge_copy().wait_send()
+        for n in range(PARTS):
+            whole_copy(n).wait_send()
+        for m in range(per):
+            own_piece(0, m).wait_send()
+
+        @pl.loop(1, team)
+        def _(j):
+            mix_copy(j).wait_send()
+            handed(j).wait_send()
+            for m in range(per):
+                piece_copy(0, j, m).wait_send()
+
+        for i in range(1, LAYERS):
+            layer_copy(i).wait_send()
+
     for store in stores:
         store.wait()
 
 
 def expert_pass(
-    stream, out_grad, ids, weights, gate_in, conv_gate, conv_value, taps, w_gate, w_up, w_down
+    fused,
+    stream,
+    out_grad,
+    ids,
+    weights,
+    gate_in,
+    conv_gate,
+    conv_value,
+    taps,
+    w_gate,
+    w_up,
+    w_down,
+    w_out,
 ):
     toks, width = stream.shape
     chans = gate_in.shape[1]
@@ -636,22 +805,26 @@
     slots = team * cap
     tall = LAYERS * slots
     deep, hid = w_gate.shape[1:]
-    crew = team_size(count)
+    blk = deep // count
+    if fused:
+        extra = (((blk, chans), F32),) + (((toks, chans), BF16),) * 3
+    else:
+        extra = (((toks, chans), F32), ((toks, chans), BF16)) + (((8, chans), F32),) * 2
+    crew = team if fused else 1
     vmem = pl.BlockSpec(memory_space=pltpu.VMEM)
     anywhere = pl.BlockSpec(memory_space=pl.ANY)
     dma = pltpu.SemaphoreType.DMA
     return pl.pallas_call(
-        functools.partial(expert_kernel, count, cap),
+        functools.partial(expert_kernel, count, cap, fused),
         out_shape=(
             jax.ShapeDtypeStruct((toks, width), BF16),
-            jax.ShapeDtypeStruct((toks, chans), F32),
-            jax.ShapeDtypeStruct((crew * toks, chans), BF16),
             jax.ShapeDtypeStruct((1, deep, hid), BF16),
             jax.ShapeDtypeStruct((1, deep, hid), BF16),
             jax.ShapeDtypeStruct((1, hid, deep), BF16),
-        ),
-        in_specs=[vmem] * 8 + [anywhere] * 3,
-        out_specs=(vmem, vmem, vmem, anywhere, anywhere, anywhere),
+        )
+        + tuple(jax.ShapeDtypeStruct(*one) for one in extra),
+        in_specs=[vmem] * 8 + [anywhere] * 4,
+        out_specs=(vmem,) + (anywhere,) * 3 + (vmem,) * 4,
         scratch_shapes=[
             pltpu.VMEM((2, LAYERS - 1, toks, width), BF16),
             pltpu.VMEM((LAYERS, 8, toks), F32),
@@ -681,9 +854,17 @@
             pltpu.VMEM((crew * toks, chans), BF16),
             pltpu.VMEM((toks, chans), BF16),
             pltpu.VMEM((toks + 8, chans), F32),
+            pltpu.VMEM((toks, chans), F32),
             pltpu.VMEM((8, chans), F32),
             pltpu.VMEM((8, chans), F32),
-            dma((3,)),
+            pltpu.VMEM((deep, chans) if fused else (16, 128), BF16),
+            pltpu.VMEM((toks, width) if fused else (16, 128), BF16),
+            pltpu.VMEM((team * toks, LAYERS * blk) if fused else (16, 128), BF16),
+            pltpu.VMEM((LAYERS, blk, chans), BF16),
+            pltpu.VMEM((LAYERS, blk, chans), BF16),
+            pltpu.VMEM((8, chans), F32),
+            pltpu.VMEM((8, chans), F32),
+            dma((4,)),
             dma((3,)),
             dma((2, 5, CHUNKS)),
             dma((2, LAYERS - 1, CHUNKS)),
@@ -702,221 +883,88 @@
             dma((crew,)),
             dma((crew,)),
             dma((2,)),
+            dma((team, LAYERS // 2)),
+            dma((team, LAYERS // 2)),
+            dma((2, LAYERS // 2)),
+            dma((team,)),
+            dma((team,)),
+            dma((LAYERS,)),
+            dma((LAYERS,)),
+            dma((PARTS,)),
+            dma((PARTS,)),
+            dma((2,)),
         ],
         compiler_params=pltpu.CompilerParams(
             collective_id=0, has_side_effects=True, vmem_limit_bytes=62 * 1024 * 1024
         ),
-    )(stream, out_grad, ids, weights, gate_in, conv_gate, conv_value, taps, w_gate, w_up, w_down)
-
-
-def mixer_kernel(
-    count,
-    sh,
-    w_out_hbm,
-    mix,
-    gate_in,
-    wog_out,
-    mg_out,
-    halo_out,
-    far,
-    w_out,
-    sg,
-    p_send,
-    p_recv,
-    h_send,
-    h_recv,
-    w_sem,
-    whole_sem,
-    gsend_sem,
-    grecv_sem,
-    fsend_sem,
-    frecv_sem,
-    own_sem,
-    psend_sem,
-    precv_sem,
-    hsem,
-):
-    me = lax.axis_index("sp")
-    half = lax.axis_index("tp")
-    other = 1 - half
-    team = team_size(count)
-    layers = count // team
-    place, layer = lax.rem(me, team), me // team
-    toks, width = sh.shape
-    per = layers // 2
-    blk = width // (team * per)
-    load = pltpu.make_async_copy(w_out_hbm, w_out, w_sem)
-    load.start()
-
-    def member(j):
-        return me - place + lax.rem(place + j, team)
-
-    def floor(i):
-        return lax.rem(layer + i, layers) * team + place
-
-    after, before = lax.rem(me + 1, count), lax.rem(me + count - 1, count)
-    barrier = pltpu.get_barrier_semaphore()
-
-    def greet(device):
-        pl.semaphore_signal(barrier, inc=1, device_id=device, device_id_type=MESH)
-
-    for j in range(1, team):
-        greet((member(j), half))
-    for i in range(1, layers):
-        greet((floor(i), half))
-    greet((me, other))
-    greet((after, half))
-    greet((before, half))
-    pl.semaphore_wait(barrier, team - 1 + layers - 1 + 3)
-
-    def remote(src, dst, send, recv, device):
-        return pltpu.make_async_remote_copy(
-            src_ref=src,
-            dst_ref=dst,
-            send_sem=send,
-            recv_sem=recv,
-            device_id=device,
-            device_id_type=MESH,
-        )
-
-    def cols(j, m):
-        at = (lax.rem(place + j, team) + team * m) * blk
-        return pl.ds(pl.multiple_of(at, blk), blk)
-
-    def spot(h, m, size):
-        return pl.ds(pl.multiple_of((h * per + m) * blk, blk), size)
-
-    def stripe(j):
-        return pl.ds(j * toks, toks)
-
-    def piece(j, m):
-        return remote(
-            sh.at[:, cols(j, m)],
-            sg.at[stripe(j), spot(half, m, blk)],
-            gsend_sem.at[j, m],
-            grecv_sem.at[j, m],
-            (member(j), half),
-        )
-
-    def own_piece(m):
-        return remote(
-            sh.at[:, cols(0, m)],
-            sg.at[stripe(0), spot(half, m, blk)],
-            own_sem.at[0, m],
-            own_sem.at[1, m],
-            (me, other),
-        )
-
-    def handed(j):
-        ref = sg.at[stripe(j), spot(half, 0, per * blk)]
-        return remote(ref, ref, fsend_sem.at[j], frecv_sem.at[j], (me, other))
-
-    whole = remote(sh, far, whole_sem.at[0], whole_sem.at[1], (me, other))
-    whole.start()
-    for j in range(1, team):
-        for m in range(per):
-            piece(j, m).start()
-    for m in range(per):
-        own_piece(m).start()
-        sg[stripe(0), spot(half, m, blk)] = sh[:, cols(0, m)]
-
-    load.wait()
-    near_at = pl.ds(pl.multiple_of(half * width, width), width)
-    far_at = pl.ds(pl.multiple_of(other * width, width), width)
-    grad = dot(sh[...], w_out[near_at], 1, 0)
-    whole.wait_recv()
-    grad = (grad + dot(far[...], w_out[far_at], 1, 0)).astype(BF16)
-    mg_out[...] = grad
-    h_send[...] = grad[:8].astype(F32) * gate_in[:8].astype(F32)
-    halo = remote(h_send, h_recv, hsem.at[0], hsem.at[1], (before, half))
-    halo.start()
-    for j in range(1, team):
-        for m in range(per):
-            piece(j, m).wait_recv()
-        handed(j).start()
-    for m in range(per):
-        own_piece(m).wait_recv()
-    for j in range(1, team):
-        handed(j).wait_recv()
-
-    def share(i):
-        at = pl.ds(pl.multiple_of(lax.rem(layer + i, layers) * blk, blk), blk)
-        return dot(sg[:, at].T, mix[...], 1, 0)
-
-    def part(i):
-        return remote(
-            p_send.at[i], p_recv.at[i], psend_sem.at[i], precv_sem.at[i], (floor(i), half)
-        )
-
-    @pl.loop(1, layers)
-    def _(i):
-        p_send[i] = share(i).astype(BF16)
-        part(i).start()
-
-    wog_out[...] = share(0)
-    for m in range(per):
-        own_piece(m).wait_send()
-    whole.wait_send()
-    for j in range(1, team):
-        for m in range(per):
-            piece(j, m).wait_send()
-        handed(j).wait_send()
-    halo.wait_send()
-    halo.wait_recv()
-    halo_out[...] = h_recv[...]
-
-    @pl.loop(1, layers)
-    def _(i):
-        part(i).wait_recv()
-        wog_out[...] += p_recv[i].astype(F32)
-
-    @pl.loop(1, layers)
-    def _(i):
-        part(i).wait_send()
-
-
-def mixer_pass(stream_half, w_out, mix, gate_in):
-    count = lax.axis_size("sp")
-    team = team_size(count)
-    layers = count // team
-    per = layers // 2
-    toks, width = stream_half.shape
-    deep, chans = w_out.shape
-    blk = deep // count
-    vmem = pl.BlockSpec(memory_space=pltpu.VMEM)
+    )(
+        stream,
+        out_grad,
+        ids,
+        weights,
+        gate_in,
+        conv_gate,
+        conv_value,
+        taps,
+        w_gate,
+        w_up,
+        w_down,
+        w_out,
+    )
+
+
+def publish_kernel(small, large, *refs):
+    total = small + large
+    ins, outs, refs = refs[:total], refs[total : 2 * total], refs[2 * total :]
+    held, wide, (in_sem, out_sem) = refs[:total], refs[total : total + large], refs[total + large :]
+
+    def spots(k):
+        if k < small:
+            return [(0, slice(None), slice(None))]
+        size = held[k].shape[0] // PARTS
+        return [(n, (0, pl.ds(n * size, size)), pl.ds(n * size, size)) for n in range(PARTS)]
+
+    def load(k, n, outer_at, at):
+        src = ins[k] if k < small else ins[k].at[outer_at]
+        dst = held[k] if k < small else held[k].at[at]
+        return pltpu.make_async_copy(src, dst, in_sem.at[k, n])
+
+    def store(k, n, outer_at, at):
+        src = held[k] if k < small else wide[k - small].at[at]
+        dst = outs[k] if k < small else outs[k].at[outer_at]
+        return pltpu.make_async_copy(src, dst, out_sem.at[k, n])
+
+    order = list(range(small, total)) + list(range(small))
+    steps = [(k, *spot) for k in order for spot in spots(k)]
+    for step in steps:
+        load(*step).start()
+    for step in steps:
+        load(*step).wait()
+        k, at = step[0], step[3]
+        if k >= small:
+            wide[k - small][at] = held[k][at].astype(F32)
+        store(*step).start()
+    for step in steps:
+        store(*step).wait()
+
+
+def publish(smalls, larges):
+    anywhere = pl.BlockSpec(memory_space=pl.ANY)
     dma = pltpu.SemaphoreType.DMA
+    total = len(smalls) + len(larges)
+    outs = [jax.ShapeDtypeStruct(x.shape, x.dtype) for x in smalls]
+    outs += [jax.ShapeDtypeStruct(x.shape, F32) for x in larges]
     return pl.pallas_call(
-        functools.partial(mixer_kernel, count),
-        out_shape=(
-            jax.ShapeDtypeStruct((blk, chans), F32),
-            jax.ShapeDtypeStruct((toks, chans), BF16),
-            jax.ShapeDtypeStruct((8, chans), F32),
-        ),
-        in_specs=[vmem, pl.BlockSpec(memory_space=pl.ANY), vmem, vmem],
-        out_specs=(vmem, vmem, vmem),
-        scratch_shapes=[
-            pltpu.VMEM((toks, width), BF16),
-            pltpu.VMEM((deep, chans), BF16),
-            pltpu.VMEM((team * toks, layers * blk), BF16),
-            pltpu.VMEM((layers, blk, chans), BF16),
-            pltpu.VMEM((layers, blk, chans), BF16),
-            pltpu.VMEM((8, chans), F32),
-            pltpu.VMEM((8, chans), F32),
-            dma,
-            dma((2,)),
-            dma((team, per)),
-            dma((team, per)),
-            dma((team,)),
-            dma((team,)),
-            dma((2, per)),
-            dma((layers,)),
-            dma((layers,)),
-            dma((2,)),
-        ],
-        compiler_params=pltpu.CompilerParams(
-            collective_id=1, has_side_effects=True, vmem_limit_bytes=32 * 1024 * 1024
-        ),
-    )(stream_half, w_out, mix, gate_in)
+        functools.partial(publish_kernel, len(smalls), len(larges)),
+        out_shape=tuple(outs),
+        in_specs=[anywhere] * total,
+        out_specs=(anywhere,) * total,
+        scratch_shapes=[pltpu.VMEM(x.shape, x.dtype) for x in smalls]
+        + [pltpu.VMEM(x.shape[1:], BF16) for x in larges]
+        + [pltpu.VMEM(x.shape[1:], F32) for x in larges]
+        + [dma((total, PARTS)), dma((total, PARTS))],
+        compiler_params=pltpu.CompilerParams(vmem_limit_bytes=62 * 1024 * 1024),
+    )(*smalls, *larges)
 
 
 def shards(
@@ -933,11 +981,12 @@
     w_up,
     w_down,
 ):
-    tok_rows = stream.shape[0]
+    tok_rows, channels = conv_gate.shape
     me = lax.axis_index("sp")
     depth = taps.shape[0]
-    channels = conv_gate.shape[1]
-    stream_half, conv_sum, mix, gate_w_grad, up_w_grad, down_w_grad = expert_pass(
+    fused = w_out.shape[0] // lax.axis_size("sp") % 128 == 0
+    stream_half, gate_w_grad, up_w_grad, down_w_grad, *extra = expert_pass(
+        fused,
         stream,
         out_grad,
         route_ids.T,
@@ -949,17 +998,20 @@
         w_gate,
         w_up,
         w_down,
+        w_out,
     )
-    if w_out.shape[0] // lax.axis_size("sp") % 128 == 0:
-        out_proj_grad, mixer_grad, halo = mixer_pass(stream_half, w_out, mix, gate_in)
-    else:
-        stream_whole = lax.all_gather(stream_half, "tp", axis=1, tiled=True)
-        mixer_grad = dot(stream_whole, w_out, 1, 0).astype(BF16)
-        out_proj_grad = lax.psum_scatter(
-            dot(stream_whole, mix[:tok_rows], 0, 0).astype(BF16), "sp", scatter_dimension=0, tiled=True
-        ).astype(F32)
-        first = mixer_grad[: depth - 1].astype(F32) * gate_in[: depth - 1].astype(F32)
-        halo = passed_along(first, "sp", -1)
+    if fused:
+        out_proj_grad, *chan_grads = extra
+        smalls = (stream_half, *chan_grads, out_proj_grad)
+        return publish(smalls, (gate_w_grad, up_w_grad, down_w_grad))
+    conv_sum, mixer_out = extra[:2]
+    stream_whole = lax.all_gather(stream_half, "tp", axis=1, tiled=True)
+    mixer_grad = dot(stream_whole, w_out, 1, 0).astype(BF16)
+    out_proj_grad = lax.psum_scatter(
+        dot(stream_whole, mixer_out, 0, 0).astype(BF16), "sp", scatter_dimension=0, tiled=True
+    ).astype(F32)
+    first = mixer_grad[: depth - 1].astype(F32) * gate_in[: depth - 1].astype(F32)
+    halo = passed_along(first, "sp", -1)
     mixer_wide = mixer_grad.astype(jnp.float32)
     gate_in_grad = (mixer_wide * conv_sum).astype(jnp.bfloat16)
     conv_inner = mixer_wide * gate_in.astype(jnp.float32)

time: 166 us -> 147 us (0.89)
  other arithmetic: 10.3 us -> 0 us
  local copies, waits for them, and re-layouts: 6.19 us -> 0 us
  Pallas kernels: 147 us -> 144 us
    convert_element_type x5 -> x0, other arithmetic: 9.44 us -> none  [the longest x1 2.61 us: shards(): gate_w_grad.astype(F32)]
    unnamed x22 -> x0, local copies, waits for them, and re-layouts: 5.37 us -> none
    pallas_call x2, Pallas kernels: 147 us -> 144 us  [the longest x1 136 us: expert_pass(): pl.pallas_call(functools.partial(expert_kernel, count, cap, fused), out_s...]
where the time goes in v2:
time: 147 us; the launch traced here: 145 us
  Pallas kernels  144 us (98%)
    pallas_call x1, Pallas kernels, expert_pass(): pl.pallas_call(functools.partial(expert_kernel, count, cap, fused), out_s...  136 us
    pallas_call x1, Pallas kernels, publish(): pl.pallas_call(functools.partial(publish_kernel, len(smalls), len(larges)...  7.54 us

profile of v2, /device:TPU:29, one launch (start us, length us, event | category | flops | bytes accessed | tf_op | source)
XLA Modules:
  0.0 144.8 jit_solution(7420710324396043190)
XLA Ops:
  0.6 136.4 %shard_map.179 = (bf16[256,1024]{1,0:T(8,128)(2,1)}, bf16[1,2048,512]{2,1,0:T(8,128)(2,1)}, bf16[1,2048,512]{2,1,0:T(8,128)(2,1)}, bf16[1,512,2048]{2,1,0:T(8,12...) custom-call(bf16[256,1024]{1,0:T(8,128)(2,1)} %stream_in.1, ...), custom_call_target="tpu_custom_call" | custom-call | tf_op jit(solution)/shard_map/pallas_call | solution.py:817
  137.1 7.5 %shard_map.180 = (bf16[256,1024]{1,0:T(8,128)(2,1)}, bf16[256,512]{1,0:T(8,128)(2,1)}, bf16[256,512]{1,0:T(8,128)(2,1)}, bf16[256,512]{1,0:T(8,128)(2,1)}, f32[1...) custom-call(bf16[256,1024]{1,0:T(8,128)(2,1)} %get-tuple-element.16.refs_0_, ...), custom_call_target="tpu_custom_call" | custom-call | tf_op jit(solution)/shard_map/pallas_call | solution.py:957

commit v3 on v2

--- a/solution.py
+++ b/solution.py
@@ -30,6 +30,26 @@
     count,
     cap,
     fused,
+    stream_hbm,
+    grad_hbm,
+    ids_hbm,
+    weights_hbm,
+    gate_hbm,
+    conv_gate_hbm,
+    conv_value_hbm,
+    taps_hbm,
+    wg_hbm,
+    wu_hbm,
+    wd_hbm,
+    wo_hbm,
+    half_hbm,
+    gate_out,
+    up_out,
+    down_out,
+    first_hbm,
+    second_hbm,
+    third_hbm,
+    fourth_hbm,
     stream_in,
     grad_in,
     ids,
@@ -38,14 +58,7 @@
     conv_gate,
     conv_value,
     taps,
-    wg_hbm,
-    wu_hbm,
-    wd_hbm,
-    wo_hbm,
     half_out,
-    gate_out,
-    up_out,
-    down_out,
     first_out,
     second_out,
     third_out,
@@ -88,6 +101,7 @@
     share_in,
     edge_src,
     edge_dst,
+    in_sem,
     w_sem,
     out_sem,
     z_send,
@@ -140,6 +154,21 @@
     def teammate(i):
         return layer * team + lax.rem(place + i, team)
 
+    firsts = []
+    for n, (a, b) in enumerate(
+        (
+            (conv_gate_hbm, conv_gate),
+            (conv_value_hbm, conv_value),
+            (stream_hbm, stream_in),
+            (ids_hbm, ids),
+            (weights_hbm, weights),
+            (grad_hbm, grad_in),
+            (gate_hbm, gate_in),
+            (taps_hbm, taps),
+        )
+    ):
+        firsts.append(pltpu.make_async_copy(a, b, in_sem.at[n]))
+        firsts[-1].start()
     loads = []
     for n, (a, b) in enumerate(((wg_hbm, wg), (wu_hbm, wu), (wd_hbm, wd))):
         load = pltpu.make_async_copy(a.at[0], b, w_sem.at[n])
@@ -167,6 +196,8 @@
     greet((me, other))
     greet((after, half))
     greet((before, half))
+    for load in firsts:
+        load.wait()
     pl.semaphore_wait(barrier, LAYERS - 1 + team - 1 + 3)
 
     def remote(src, dst, send, recv, device):
@@ -193,14 +224,14 @@
     def blocks_of(which, j):
         return whole[which] if j == OWN else toks_in.at[which, j - 1]
 
-    stretch = toks // CHUNKS
+    stretch = width // CHUNKS
 
     def hop(which, n, j, to, lands, c):
         at = pl.ds(c * stretch, stretch)
         return remote(
-            blocks_of(which, j).at[at],
-            toks_in.at[which, lands - 1, at],
-            z_send.at[which, n, c],
+            blocks_of(which, j).at[:, at],
+            toks_in.at[which, lands - 1, :, at],
+            z_send.at[which, n],
             z_recv.at[which, lands - 1, c],
             column(to),
         )
@@ -289,44 +320,65 @@
 
     bufs = (rows, cot)
 
-    def in_copy(which, j, i):
-        return remote(
-            rel.at[which, j, block(lax.rem(place + i, team))],
-            bufs[which].at[half, piece(j, place)],
-            i_send.at[which, j, i],
+    def in_copy(which, j, i, at=slice(None)):
+        return remote(
+            rel.at[which, j, block(lax.rem(place + i, team)), at],
+            bufs[which].at[half, piece(j, place), at],
+            i_send.at[which, j],
             i_recv.at[which, j, i],
             (teammate(i), half),
         )
 
     def in_arrival(which, j, i):
         at = bufs[which].at[half, piece(j, lax.rem(place - i + team, team))]
-        return remote(at, at, i_send.at[which, j, i], i_recv.at[which, j, i], (teammate(i), half))
+        return remote(at, at, i_send.at[which, j], i_recv.at[which, j, i], (teammate(i), half))
 
     def pass_copy(which, j, i):
         at = bufs[which].at[half, piece(j, lax.rem(place - i + team, team))]
-        return remote(at, at, f_send.at[which, j, i], f_recv.at[which, j, i], (me, other))
+        return remote(at, at, f_send.at[which, j], f_recv.at[which, j], (me, other))
 
     def own_pass(which, j):
         return remote(
             rel.at[which, j, block(place)],
             bufs[which].at[half, piece(j, place)],
-            f_send.at[which, j, 0],
-            f_recv.at[which, j, 0],
+            f_send.at[which, j],
+            f_recv.at[which, j],
             (me, other),
         )
 
-    def deal(which, j):
-        chosen = dot(pick[j], blocks_of(which, j)[...], 1, 0)
+    def passed(which, j):
+        at = bufs[which].at[half, group(j)]
+        return remote(at, at, f_send.at[which, j], f_recv.at[which, j], (me, other))
+
+    def dealt(which, j):
+        at = bufs[which].at[half, pl.ds(j * slots, slots - cap)]
+        return remote(at, at, i_send.at[which, j], i_recv.at[which, j, 0], (me, other))
+
+    def deal_chunk(which, j, c):
+        at = pl.ds(c * stretch, stretch)
+        chosen = dot(pick[j], blocks_of(which, j)[:, at], 1, 0)
         if which == 1:
             chosen = scale[j] * chosen
-        rel[which, j] = chosen.astype(BF16)
+        rel[which, j, :, at] = chosen.astype(BF16)
 
         @pl.loop(1, team)
         def _(i):
-            in_copy(which, j, i).start()
-
+            in_copy(which, j, i, at).start()
+
+    def deal_own(which, j):
         own_pass(which, j).start()
         bufs[which][half, piece(j, place)] = rel[which, j, block(place)]
+
+    def deal(which, j):
+        for c in range(CHUNKS):
+            deal_chunk(which, j, c)
+        deal_own(which, j)
+
+    def deal_arriving(which, j):
+        for c in range(CHUNKS):
+            hop(which, 0, j, next_layer, j, c).wait_recv()
+            deal_chunk(which, j, c)
+        deal_own(which, j)
 
     def gather(which, j):
         @pl.loop(1, team)
@@ -334,9 +386,7 @@
             in_arrival(which, j, i).wait_recv()
             pass_copy(which, j, i).start()
 
-        @pl.loop(0, team)
-        def _(i):
-            pass_copy(which, j, i).wait_recv()
+        passed(which, j).wait_recv()
 
     mine_at = pl.ds(pl.multiple_of(half * width, width), width)
     other_at = pl.ds(pl.multiple_of(other * width, width), width)
@@ -350,14 +400,14 @@
         return remote(
             ret.at[piece(j, lax.rem(place + i, team))],
             back.at[piece(j, place)],
-            r_send.at[j, i],
-            r_recv.at[j, i],
+            r_send.at[j],
+            r_recv.at[j],
             (teammate(i), half),
         )
 
-    def ret_arrival(j, i):
-        at = back.at[piece(j, lax.rem(place - i + team, team))]
-        return remote(at, at, r_send.at[j, i], r_recv.at[j, i], (teammate(i), half))
+    def ret_all(j):
+        at = back.at[pl.ds(j * slots, slots - cap)]
+        return remote(at, at, r_send.at[j], r_recv.at[j], (me, other))
 
     def ahead(j):
         gather(0, j)
@@ -386,6 +436,7 @@
         part_copy(j).wait_recv()
         ret[at] = (near + part_in[at].astype(F32)).astype(BF16)
 
+    def send_back(j):
         @pl.loop(1, team)
         def _(i):
             ret_copy(j, i).start()
@@ -393,9 +444,7 @@
         back[piece(j, place)] = ret[piece(j, place)]
 
     def returned(j):
-        @pl.loop(1, team)
-        def _(i):
-            ret_arrival(j, i).wait_recv()
+        ret_all(j).wait_recv()
 
     share = width // PARTS
 
@@ -411,14 +460,14 @@
         return remote(
             col_out.at[j - 1, :, cols(n)],
             col_in.at[lands, :, cols(n)],
-            c_send.at[j - 1, n],
+            c_send.at[j - 1],
             c_recv.at[lands, n],
             column(to),
         )
 
     def sum_arrival(lands, n):
         at = col_in.at[lands, :, cols(n)]
-        return remote(at, at, c_send.at[0, n], c_recv.at[lands, n], column(next_layer))
+        return remote(at, at, c_send.at[0], c_recv.at[lands, n], column(next_layer))
 
     def partial(j, n):
         return dot(pick[j], back[group(j), cols(n)], 0, 0)
@@ -454,10 +503,14 @@
         return remote(
             mix_src,
             mix.at[pl.ds(pl.multiple_of(j * toks, toks), toks)],
-            m_send.at[j],
-            m_recv.at[j],
+            m_send.at[0],
+            m_recv.at[0],
             (teammate(j), half),
         )
+
+    def mix_all():
+        at = mix.at[pl.ds(0, (team - 1) * toks)]
+        return remote(at, at, m_send.at[0], m_recv.at[0], (me, other))
 
     def informed(j):
         table_copy(0, next_layer, j).wait_recv()
@@ -488,6 +541,7 @@
     deal(1, NEXT)
     ahead(OWN)
     behind(OWN)
+    send_back(OWN)
 
     @pl.when(inner)
     def _():
@@ -495,6 +549,7 @@
 
     ahead(NEXT)
     behind(NEXT)
+    send_back(NEXT)
 
     @pl.when(outer)
     def _():
@@ -522,18 +577,26 @@
 
     @pl.when(outer)
     def _():
-        arrived(1, FAR)
-
-    deal(1, FAR)
+        deal_arriving(1, FAR)
+
+    @pl.when(inner)
+    def _():
+        deal(1, FAR)
+
     ahead(FAR)
 
     @pl.when(outer)
     def _():
-        arrived(1, ACROSS)
-
-    deal(1, ACROSS)
+        deal_arriving(1, ACROSS)
+
+    @pl.when(inner)
+    def _():
+        deal(1, ACROSS)
+
     behind(FAR)
+    send_back(FAR)
     behind(ACROSS)
+    send_back(ACROSS)
 
     if fused:
 
@@ -570,6 +633,8 @@
         @pl.when(inner)
         def _():
             forward_sum(FAR, n)
+            if n >= 2:
+                forward_sum(NEXT, n - 2)
 
         weights_part(n)
 
@@ -581,22 +646,6 @@
     for store in stores:
         store.start()
 
-    returned(ACROSS)
-
-    @pl.when(outer)
-    def _():
-        send_sums(ACROSS)
-
-    @pl.when(inner)
-    def _():
-        for n in range(PARTS):
-            forward_sum(NEXT, n)
-            forward_sum(ACROSS, n)
-
-        for n in range(PARTS):
-            sum_arrival(1, n).wait_recv()
-            total[:, cols(n)] += col_in[1, :, cols(n)].astype(F32)
-
     per = LAYERS // 2
     blk = width // (team * per)
 
@@ -613,8 +662,8 @@
         return remote(
             half_out.at[:, band(b)],
             strips.at[stripe(j), spot(half, m, blk)],
-            g_send.at[j, m],
-            g_recv.at[j, m],
+            g_send.at[m],
+            g_recv.at[m],
             (teammate(j), half),
         )
 
@@ -629,16 +678,40 @@
 
     def whole_copy(n):
         return remote(
-            half_out.at[:, cols(n)], far_half.at[:, cols(n)], b_send.at[n], b_recv.at[n], (me, other)
-        )
-
-    def handed(j):
-        at = strips.at[stripe(j), spot(half, 0, per * blk)]
-        return remote(at, at, d_send.at[j], d_recv.at[j], (me, other))
-
-    def layer_copy(i):
-        to = lax.rem(layer + i, LAYERS)
-        return remote(share_out.at[i], share_in.at[i], s_send.at[i], s_recv.at[i], column(to))
+            half_out.at[:, cols(n)], far_half.at[:, cols(n)], b_send.at[0], b_recv.at[0], (me, other)
+        )
+
+    def whole_all():
+        return remote(half_out, far_half, b_send.at[0], b_recv.at[0], (me, other))
+
+    def handed(j, m):
+        at = strips.at[stripe(j), spot(half, m, blk)]
+        return remote(at, at, d_send.at[m], d_recv.at[m], (me, other))
+
+    def layer_copy(at):
+        return remote(
+            share_out.at[at], share_in.at[layer], s_send.at[at], s_recv.at[layer], column(at)
+        )
+
+    def layer_arrival(at):
+        return remote(
+            share_in.at[at], share_in.at[at], s_send.at[at], s_recv.at[at], column(at)
+        )
+
+    def hand_over(m):
+        pieces_all(m).wait_recv()
+
+        @pl.loop(1, team)
+        def _(j):
+            handed(j, m).start()
+
+    def pieces_all(m):
+        at = strips.at[pl.ds(toks, (team - 1) * toks), band(m)]
+        return remote(at, at, g_send.at[m], g_recv.at[m], (me, other))
+
+    def handed_all(m):
+        at = strips.at[pl.ds(toks, (team - 1) * toks), band(m)]
+        return remote(at, at, d_send.at[m], d_recv.at[m], (me, other))
 
     def settle(n):
         sum_arrival(0, n).wait_recv()
@@ -658,13 +731,44 @@
                     own_piece(b, m).start()
                     strips[stripe(0), spot(half, m, blk)] = half_out[:, band(b)]
 
+    def settle_inner(n):
+        sum_arrival(1, n).wait_recv()
+        total[:, cols(n)] += col_in[1, :, cols(n)].astype(F32)
+        settle(n)
+
+    returned(ACROSS)
+
+    @pl.when(outer)
+    def _():
+        send_sums(ACROSS)
+
+    @pl.when(inner)
+    def _():
+        for n in range(PARTS):
+            forward_sum(ACROSS, n)
+            if n < 2:
+                forward_sum(NEXT, PARTS - 2 + n)
+            if n >= 2:
+                settle_inner(n - 2)
+        settle_inner(PARTS - 2)
+        if fused:
+            hand_over(0)
+        settle_inner(PARTS - 1)
+
+    @pl.when(outer)
+    def _():
+        for n in range(PARTS - 1):
+            settle(n)
+        if fused:
+            hand_over(0)
+        settle(PARTS - 1)
+
     def edge_copy():
         return remote(edge_src, edge_dst, e_sem.at[0], e_sem.at[1], (before, half))
 
     def mixer_grad():
         mixed = dot(half_out[...], wo[mine_at], 1, 0)
-        for n in range(PARTS):
-            whole_copy(n).wait_recv()
+        whole_all().wait_recv()
         mixed = (mixed + dot(far_half[...], wo[other_at], 1, 0)).astype(BF16)
         wide = mixed.astype(F32)
         inner_conv = wide * gate_in[...].astype(F32)
@@ -683,103 +787,103 @@
         third_out[...] = (prod_grad * conv_value[...].astype(F32)).astype(BF16)
         fourth_out[...] = (prod_grad * conv_gate[...].astype(F32)).astype(BF16)
 
-    def strips_in():
-        @pl.loop(1, team)
-        def _(j):
-            for m in range(per):
-                piece_copy(0, j, m).wait_recv()
-            handed(j).start()
-
-        for m in range(per):
-            own_piece(0, m).wait_recv()
-
-        @pl.loop(1, team)
-        def _(j):
-            handed(j).wait_recv()
-            mix_copy(j).wait_recv()
-
-    def layer_share(i):
-        at = pl.ds(pl.multiple_of(lax.rem(layer + i, LAYERS) * blk, blk), blk)
-        return dot(strips[:, at].T, mix[...], 1, 0)
-
-    def shares_out():
-        for i in (2, 1, 3):
-            share_out[i] = layer_share(i).astype(BF16)
-            layer_copy(i).start()
-        first_out[...] = layer_share(0)
+    def strips_in(m):
+        own_piece(0, m).wait_recv()
+        handed_all(m).wait_recv()
+
+    def shares_out(m):
+        for at in range(m, LAYERS, per):
+            now = dot(strips[:, band(at)].T, mix[...], 1, 0)
+
+            @pl.when(layer == at)
+            def _():
+                first_out[...] = now
+
+            @pl.when(layer != at)
+            def _():
+                share_out[at] = now.astype(BF16)
+                layer_copy(at).start()
 
     def shares_in():
         for i in (1, 3, 2):
-            layer_copy(i).wait_recv()
-            first_out[...] += share_in[i].astype(F32)
-
-    for n in range(PARTS):
-        settle(n)
+            at = lax.rem(layer + i, LAYERS)
+            layer_arrival(at).wait_recv()
+            first_out[...] += share_in[at].astype(F32)
+
+    def hopped(which, n):
+        at = toks_in.at[which, 0]
+        return remote(at, at, z_send.at[which, n], z_recv.at[which, 0, 0], column(next_layer))
+
+    def summed(j):
+        at = col_out.at[j - 1]
+        return remote(at, at, c_send.at[j - 1], c_recv.at[0, 0], column(next_layer))
+
+    def drain():
+        for which in range(2):
+            hopped(which, 0).wait_send()
+            for j in range(LAYERS):
+                passed(which, j).wait_send()
+                dealt(which, j).wait_send()
+
+        @pl.when(inner)
+        def _():
+            for which in range(2):
+                for n in range(1, 5):
+                    hopped(which, n).wait_send()
+
+        for j in range(LAYERS):
+            part_copy(j).wait_send()
+            ret_all(j).wait_send()
+        for j in (NEXT, ACROSS, FAR):
+            summed(j).wait_send()
+        for copy in tables:
+            copy.wait_send()
+        halo.wait_send()
+        if fused:
+            edge_copy().wait_send()
+            whole_all().wait_send()
+            mix_all().wait_send()
+            for m in range(per):
+                own_piece(0, m).wait_send()
+                handed_all(m).wait_send()
+                pieces_all(m).wait_send()
+
+    def keep(n, src, dst):
+        stores.append(pltpu.make_async_copy(src, dst, out_sem.at[n]))
+        stores[-1].start()
+
+    keep(3, half_out, half_hbm)
     if fused:
-        strips_in()
-        shares_out()
-        mixer_grad()
+
+        mix_all().wait_recv()
+        for m in range(per):
+            strips_in(m)
+            shares_out(m)
+            if m == 0:
+                mixer_grad()
+            if m + 1 < per:
+                hand_over(m + 1)
         conv_grads()
+        keep(5, second_out, second_hbm)
+        keep(6, third_out, third_hbm)
+        keep(7, fourth_out, fourth_hbm)
+        drain()
         shares_in()
+        keep(4, first_out, first_hbm)
+        for i in range(1, LAYERS):
+            layer_copy(lax.rem(layer + i, LAYERS)).wait_send()
     else:
-        first_out[...] = conv_sum[...]
-        second_out[...] = mix_src[...]
-        fourth_out[...] = jnp.zeros(fourth_out.shape, fourth_out.dtype)
-        third_out[...] = jnp.zeros(third_out.shape, third_out.dtype)
-
-    for which in range(2):
-        for c in range(CHUNKS):
-            own_to_next(which, c).wait_send()
-
-        for j in range(LAYERS):
-            own_pass(which, j).wait_send()
-
-            @pl.loop(1, team)
-            def _(i):
-                in_copy(which, j, i).wait_send()
-                pass_copy(which, j, i).wait_send()
-
-    @pl.when(inner)
-    def _():
-        for which in range(2):
-            for copy in (own_to_across, next_to_across, across_to_next, far_to_next):
-                for c in range(CHUNKS):
-                    copy(which, c).wait_send()
-
-    for j in range(LAYERS):
-        part_copy(j).wait_send()
-
-        @pl.loop(1, team)
-        def _(i):
-            ret_copy(j, i).wait_send()
-
-    for j in (NEXT, ACROSS, FAR):
-        for n in range(PARTS):
-            sum_copy(j, n).wait_send()
-
-    for copy in tables:
-        copy.wait_send()
-    halo.wait_send()
-
-    if fused:
-        edge_copy().wait_send()
-        for n in range(PARTS):
-            whole_copy(n).wait_send()
-        for m in range(per):
-            own_piece(0, m).wait_send()
-
-        @pl.loop(1, team)
-        def _(j):
-            mix_copy(j).wait_send()
-            handed(j).wait_send()
-            for m in range(per):
-                piece_copy(0, j, m).wait_send()
-
-        for i in range(1, LAYERS):
-            layer_copy(i).wait_send()
-
-    for store in stores:
-        store.wait()
+        drain()
+        keep(4, conv_sum, first_hbm)
+        keep(5, mix_src, second_hbm)
+        keep(6, halo_src, third_hbm)
+        keep(7, halo_dst, fourth_hbm)
+
+    def finish():
+        for store in stores:
+            store.wait()
+
+    finish()
 
 
 def expert_pass(
@@ -811,7 +915,6 @@
     else:
         extra = (((toks, chans), F32), ((toks, chans), BF16)) + (((8, chans), F32),) * 2
     crew = team if fused else 1
-    vmem = pl.BlockSpec(memory_space=pltpu.VMEM)
     anywhere = pl.BlockSpec(memory_space=pl.ANY)
     dma = pltpu.SemaphoreType.DMA
     return pl.pallas_call(
@@ -823,9 +926,22 @@
             jax.ShapeDtypeStruct((1, hid, deep), BF16),
         )
         + tuple(jax.ShapeDtypeStruct(*one) for one in extra),
-        in_specs=[vmem] * 8 + [anywhere] * 4,
-        out_specs=(vmem,) + (anywhere,) * 3 + (vmem,) * 4,
+        in_specs=[anywhere] * 12,
+        out_specs=(anywhere,) * 8,
         scratch_shapes=[
+            pltpu.VMEM((toks, width), BF16),
+            pltpu.VMEM((toks, width), BF16),
+            pltpu.VMEM(ids.shape, ids.dtype),
+            pltpu.VMEM(weights.shape, F32),
+            pltpu.VMEM((toks, chans), BF16),
+            pltpu.VMEM((toks, chans), BF16),
+            pltpu.VMEM((toks, chans), BF16),
+            pltpu.VMEM(taps.shape, F32),
+            pltpu.VMEM((toks, width), BF16),
+            pltpu.VMEM((blk, chans), F32),
+            pltpu.VMEM((toks, chans), BF16),
+            pltpu.VMEM((toks, chans), BF16),
+            pltpu.VMEM((toks, chans), BF16),
             pltpu.VMEM((2, LAYERS - 1, toks, width), BF16),
             pltpu.VMEM((LAYERS, 8, toks), F32),
             pltpu.VMEM((LAYERS, slots, toks), BF16),
@@ -864,34 +980,35 @@
             pltpu.VMEM((LAYERS, blk, chans), BF16),
             pltpu.VMEM((8, chans), F32),
             pltpu.VMEM((8, chans), F32),
+            dma((8,)),
             dma((4,)),
-            dma((3,)),
-            dma((2, 5, CHUNKS)),
+            dma((8,)),
+            dma((2, 5)),
             dma((2, LAYERS - 1, CHUNKS)),
             dma((3,)),
             dma((LAYERS,)),
+            dma((2, LAYERS)),
             dma((2, LAYERS, team)),
-            dma((2, LAYERS, team)),
-            dma((2, LAYERS, team)),
-            dma((2, LAYERS, team)),
+            dma((2, LAYERS)),
+            dma((2, LAYERS)),
             dma((LAYERS,)),
             dma((LAYERS,)),
-            dma((LAYERS, team)),
-            dma((LAYERS, team)),
-            dma((LAYERS - 1, PARTS)),
-            dma((5, PARTS)),
-            dma((crew,)),
-            dma((crew,)),
-            dma((2,)),
-            dma((team, LAYERS // 2)),
-            dma((team, LAYERS // 2)),
-            dma((2, LAYERS // 2)),
-            dma((team,)),
-            dma((team,)),
             dma((LAYERS,)),
             dma((LAYERS,)),
-            dma((PARTS,)),
-            dma((PARTS,)),
+            dma((LAYERS - 1,)),
+            dma((5, PARTS)),
+            dma((1,)),
+            dma((1,)),
+            dma((2,)),
+            dma((LAYERS // 2,)),
+            dma((LAYERS // 2,)),
+            dma((2, LAYERS // 2)),
+            dma((LAYERS // 2,)),
+            dma((LAYERS // 2,)),
+            dma((LAYERS,)),
+            dma((LAYERS,)),
+            dma((1,)),
+            dma((1,)),
             dma((2,)),
         ],
         compiler_params=pltpu.CompilerParams(

time: 147 us -> 140 us (0.952); the launches traced: 145 us -> 139 us
  Pallas kernels: 144 us -> 139 us
    pallas_call x1, Pallas kernels: 136 us -> 131 us  [expert_pass(): pl.pallas_call(functools.partial(expert_kernel, count, cap, fused), out_s...]
where the time goes in v3:
time: 140 us; the launch traced here: 139 us
  Pallas kernels  139 us (99%)
    pallas_call x1, Pallas kernels, expert_pass(): pl.pallas_call(functools.partial(expert_kernel, count, cap, fused), out_s...  131 us
    pallas_call x1, Pallas kernels, publish(): pl.pallas_call(functools.partial(publish_kernel, len(smalls), len(larges)...  7.54 us

profile of v3, /device:TPU:29, one launch (start us, length us, event | category | flops | bytes accessed | tf_op | source)
XLA Modules:
  0.0 139.4 jit_solution(11153434280883651300)
XLA Ops:
  0.6 131.0 %shard_map.179 = (bf16[256,1024]{1,0:T(8,128)(2,1)}, bf16[1,2048,512]{2,1,0:T(8,128)(2,1)}, bf16[1,2048,512]{2,1,0:T(8,128)(2,1)}, bf16[1,512,2048]{2,1,0:T(8,12...) custom-call(bf16[256,1024]{1,0:T(8,128)(2,1)} %stream_hbm.1, ...), custom_call_target="tpu_custom_call" | custom-call | tf_op jit(solution)/shard_map/pallas_call | solution.py:920
  131.7 7.5 %shard_map.180 = (bf16[256,1024]{1,0:T(8,128)(2,1)}, bf16[256,512]{1,0:T(8,128)(2,1)}, bf16[256,512]{1,0:T(8,128)(2,1)}, bf16[256,512]{1,0:T(8,128)(2,1)}, f32[1...) custom-call(bf16[256,1024]{1,0:T(8,128)(2,1)} %get-tuple-element.16.refs_0_, ...), custom_call_target="tpu_custom_call" | custom-call | tf_op jit(solution)/shard_map/pallas_call | solution.py:1074

commit v4 on v3

--- a/solution.py
+++ b/solution.py
@@ -396,18 +396,21 @@
             part_out.at[group(j)], part_in.at[group(j)], p_send.at[j], p_recv.at[j], (me, other)
         )
 
-    def ret_copy(j, i):
-        return remote(
-            ret.at[piece(j, lax.rem(place + i, team))],
-            back.at[piece(j, place)],
-            r_send.at[j],
-            r_recv.at[j],
+    def side_of(h):
+        return pl.ds(h * (width // 2), width // 2)
+
+    def ret_copy(j, i, h):
+        return remote(
+            ret.at[piece(j, lax.rem(place + i, team)), side_of(h)],
+            back.at[piece(j, place), side_of(h)],
+            r_send.at[j, h],
+            r_recv.at[j, h],
             (teammate(i), half),
         )
 
-    def ret_all(j):
-        at = back.at[pl.ds(j * slots, slots - cap)]
-        return remote(at, at, r_send.at[j], r_recv.at[j], (me, other))
+    def ret_all(j, h):
+        at = back.at[pl.ds(j * slots, slots - cap), side_of(h)]
+        return remote(at, at, r_send.at[j, h], r_recv.at[j, h], (me, other))
 
     def ahead(j):
         gather(0, j)
@@ -437,14 +440,17 @@
         ret[at] = (near + part_in[at].astype(F32)).astype(BF16)
 
     def send_back(j):
-        @pl.loop(1, team)
-        def _(i):
-            ret_copy(j, i).start()
+        for h in range(2):
+
+            @pl.loop(1, team)
+            def _(i):
+                ret_copy(j, i, h).start()
 
         back[piece(j, place)] = ret[piece(j, place)]
 
     def returned(j):
-        ret_all(j).wait_recv()
+        for h in range(2):
+            ret_all(j, h).wait_recv()
 
     share = width // PARTS
 
@@ -472,8 +478,10 @@
     def partial(j, n):
         return dot(pick[j], back[group(j), cols(n)], 0, 0)
 
-    def send_sums(j):
+    def send_sums(j, fresh=False):
         for n in range(PARTS):
+            if fresh and n % (PARTS // 2) == 0:
+                ret_all(j, n // (PARTS // 2)).wait_recv()
             col_out[j - 1, :, cols(n)] = partial(j, n).astype(BF16)
             sum_copy(j, n).start()
 
@@ -606,11 +614,13 @@
 
         mix[pl.ds(0, toks)] = mix_src[...]
 
-    returned(FAR)
+    @pl.when(inner)
+    def _():
+        returned(FAR)
 
     @pl.when(outer)
     def _():
-        send_sums(FAR)
+        send_sums(FAR, True)
 
     hid_part = hidden.shape[1] // PARTS
     deep_part = width // PARTS
@@ -736,14 +746,13 @@
         total[:, cols(n)] += col_in[1, :, cols(n)].astype(F32)
         settle(n)
 
-    returned(ACROSS)
-
     @pl.when(outer)
     def _():
-        send_sums(ACROSS)
+        send_sums(ACROSS, True)
 
     @pl.when(inner)
     def _():
+        returned(ACROSS)
         for n in range(PARTS):
             forward_sum(ACROSS, n)
             if n < 2:
@@ -833,7 +842,9 @@
 
         for j in range(LAYERS):
             part_copy(j).wait_send()
-            ret_all(j).wait_send()
+            for h in range(2):
+                ret_all(j, h).wait_send()
+
         for j in (NEXT, ACROSS, FAR):
             summed(j).wait_send()
         for copy in tables:
@@ -993,8 +1004,8 @@
             dma((2, LAYERS)),
             dma((LAYERS,)),
             dma((LAYERS,)),
-            dma((LAYERS,)),
-            dma((LAYERS,)),
+            dma((LAYERS, 2)),
+            dma((LAYERS, 2)),
             dma((LAYERS - 1,)),
             dma((5, PARTS)),
             dma((1,)),

time: 140 us -> 138 us (0.986)
  Pallas kernels: 139 us -> 137 us
    pallas_call x1, Pallas kernels: 131 us -> 129 us  [expert_pass(): pl.pallas_call(functools.partial(expert_kernel, count, cap, fused), out_s...]
where the time goes in v4:
time: 138 us
  Pallas kernels  137 us (99%)
    pallas_call x1, Pallas kernels, expert_pass(): pl.pallas_call(functools.partial(expert_kernel, count, cap, fused), out_s...  129 us
    pallas_call x1, Pallas kernels, publish(): pl.pallas_call(functools.partial(publish_kernel, len(smalls), len(larges)...  7.54 us

profile of v4, /device:TPU:29, one launch (start us, length us, event | category | flops | bytes accessed | tf_op | source)
XLA Modules:
  0.0 137.7 jit_solution(7016746309000608745)
XLA Ops:
  0.6 129.3 %shard_map.179 = (bf16[256,1024]{1,0:T(8,128)(2,1)}, bf16[1,2048,512]{2,1,0:T(8,128)(2,1)}, bf16[1,2048,512]{2,1,0:T(8,128)(2,1)}, bf16[1,512,2048]{2,1,0:T(8,12...) custom-call(bf16[256,1024]{1,0:T(8,128)(2,1)} %stream_hbm.1, ...), custom_call_target="tpu_custom_call" | custom-call | tf_op jit(solution)/shard_map/pallas_call | solution.py:931
  130.0 7.5 %shard_map.180 = (bf16[256,1024]{1,0:T(8,128)(2,1)}, bf16[256,512]{1,0:T(8,128)(2,1)}, bf16[256,512]{1,0:T(8,128)(2,1)}, bf16[256,512]{1,0:T(8,128)(2,1)}, f32[1...) custom-call(bf16[256,1024]{1,0:T(8,128)(2,1)} %get-tuple-element.16.refs_0_, ...), custom_call_target="tpu_custom_call" | custom-call | tf_op jit(solution)/shard_map/pallas_call | solution.py:1085
